TPU v7x, 512 devices: a whole 4x8x8 slice. The times are simulated.
512 devices in a mesh: ep: 32 (over z, x), tp: 16 (over y, core).
Axes of the slice: x: 4, y: 8, z: 8, core: 2. Of those that a mesh axis runs over, the one named last changes fastest.
Arguments:
- query_rows: bfloat16 [12288, 4096], P('ep', 'tp'), may hold values from -6 to 6
- key_rows: bfloat16 [12288, 2048], P('ep', 'tp'), may hold values from -6 to 6
- value_rows: bfloat16 [12288, 2048], P('ep', 'tp'), may hold values from -6 to 6
- query_gain: float32 [128], replicated, may hold values from 0.4 to 5
- key_gain: float32 [128], replicated, may hold values from 0.4 to 5
- w_out: bfloat16 [4096, 2048], P('tp'), may hold values from -0.09375 to 0.09375
- mixer_gain: float32 [2048], replicated, may hold values from 0.1 to 1.9
- expert_input: bfloat16 [6144, 2048], P('ep'), may hold values from -6 to 6
- expert_ids: int32 [6144, 2], P('ep'), may hold values from 0 to 31, as said below
- expert_weights: float32 [6144, 2], P('ep'), may hold values from 0.1 to 1
- input_gain: float32 [2048], replicated, may hold values from 0.1 to 1.9
- w_gate: bfloat16 [32, 2048, 4096], P('ep', None, 'tp'), may hold values from -0.125 to 0.125
- w_up: bfloat16 [32, 2048, 4096], P('ep', None, 'tp'), may hold values from -0.125 to 0.125
- w_down: bfloat16 [32, 4096, 2048], P('ep', 'tp'), may hold values from -2 to 2
- out_gain: float32 [2048], P('tp'), may hold values from 0.1 to 1.9
Outputs:
- mixer_result: bfloat16 [12288, 2048], P(('ep', 'tp'))
- moe_result: bfloat16 [6144, 2048], P('ep', 'tp')
Inputs may be any that keep to these rules, and one draw needn't show every extreme that they name: `expert_ids`: the two experts of a row differ and lie in one group of 8 consecutive experts. Among the rows of one index of ep (aligned blocks of 192 rows) no expert is named by more than 18 rows, and in every block some expert is named by exactly 18 rows.
All inputs are finite; a program needn't handle non-finite values.
Results may differ from a plain program's by a relative error of at most 0.02.
The roundings to bfloat16 on the way count: a program that leaves them out, or rounds other values in their place, can miss the bound.
Values may be sent and summed in bfloat16 or wider, within the bound.
A program may use at most 64 MiB of HBM per device.

v0:
```python
import jax
import jax.numpy as jnp
from jax import lax
from jax.sharding import Mesh
from jax.sharding import PartitionSpec as P

D = 2048
GRID = 64
GROUPS = 4
TP = ("tp_0", "tp_1")
EP_TP = ("ep", "tp_0", "tp_1")


EPS = 1e-06
THETA = 10000.0


def sent_together(arrays, axis, dim, along):
    ends, at = ([], 0)
    for a in arrays[:-1]:
        at += a.shape[along]
        ends.append(at)
    both = jnp.concatenate(arrays, axis=along)
    return tuple(jnp.split(lax.all_gather(both, axis, axis=dim, tiled=True), ends, axis=along))


def sum_by_axis(terms, axes):
    running = terms.astype(jnp.bfloat16)
    for axis in axes:
        running = lax.psum_scatter(running, axis, scatter_dimension=0, tiled=True)
    return running.astype(jnp.float32)


def sent_to_all(shard, axis):
    count = lax.axis_size(axis)
    return lax.all_to_all(
        jnp.broadcast_to(shard[None], (count, *shard.shape)), axis, 0, 0, tiled=True
    )


def joined_along(blocks, dim):
    lengths = list(blocks.shape[1:])
    lengths[dim] *= blocks.shape[0]
    return jnp.moveaxis(blocks, 0, dim).reshape(lengths)


def gathered_copies(shard, axis, dim):
    blocks = sent_to_all(shard, axis)
    return joined_along(blocks, dim)


def split_up(shard, dim, count):
    lengths = shard.shape
    blocks = shard.reshape(*lengths[:dim], count, lengths[dim] // count, *lengths[dim + 1 :])
    return jnp.moveaxis(blocks, dim, 0)


def sent_and_summed(shard, axis, dim):
    blocks = split_up(shard, dim, lax.axis_size(axis))
    arrived = lax.all_to_all(blocks, axis, split_axis=0, concat_axis=0, tiled=True)
    return arrived.astype(jnp.float32).sum(axis=0)


def taken_together(shard, axis):
    return sent_to_all(shard, axis).sum(axis=0)


def turn_half(half_part, position):
    half_width = half_part.shape[-1]
    frequency = THETA ** (-jnp.arange(0, half_width, 2, dtype=jnp.float32) / half_width)
    angles = position[:, None, None] * frequency[None, None, :]
    cosine = jnp.cos(angles)
    sine_part = jnp.sin(angles)
    first_half = half_part[..., : half_width // 2]
    second = half_part[..., half_width // 2 :]
    return jnp.concatenate(
        [first_half * cosine - second * sine_part, second * cosine + first_half * sine_part],
        axis=-1,
    )


def norm_turn(raw_rows, gain_vec, row_offset):
    row_count = raw_rows.shape[0]
    head_dim = gain_vec.shape[0]
    head_count = raw_rows.shape[1] // head_dim
    by_head = raw_rows.astype(jnp.float32).reshape(row_count, head_count, head_dim)
    scaled = (
        by_head * lax.rsqrt(jnp.mean(by_head * by_head, axis=-1, keepdims=True) + EPS) * gain_vec
    )
    position = row_offset + jnp.arange(row_count, dtype=jnp.int32)
    grid_row = (position // GRID).astype(jnp.float32)
    grid_col = (position % GRID).astype(jnp.float32)
    half_dim = head_dim // 2
    turned = jnp.concatenate(
        [turn_half(scaled[..., :half_dim], grid_row), turn_half(scaled[..., half_dim:], grid_col)],
        axis=-1,
    )
    return turned.reshape(row_count, head_count * head_dim).astype(jnp.bfloat16)


def mixer_half(query_rows, key_rows, value_rows, query_gain, key_gain, w_out, mixer_gain):
    row_count = query_rows.shape[0]
    head_dim = query_gain.shape[0]
    row_offset = lax.axis_index("ep") * row_count
    query_turned = norm_turn(query_rows, query_gain, row_offset)
    key_turned = norm_turn(key_rows, key_gain, row_offset)
    local_kv = key_rows.shape[1] // head_dim
    group_size = query_rows.shape[1] // key_rows.shape[1]
    lane_count = group_size * row_count
    grouped = (
        query_turned.reshape(row_count, local_kv, group_size, head_dim)
        .transpose(1, 2, 0, 3)
        .reshape(local_kv, lane_count, head_dim)
    )
    scaling = head_dim ** (-0.5)

    def attend_block(carry, block_pair):
        running_max, running_sum, weighted = carry
        key_block, value_block = block_pair
        scores = (
            jnp.einsum("gqd,ngd->gqn", grouped, key_block, preferred_element_type=jnp.float32)
            * scaling
        )
        new_max = jnp.maximum(running_max, jnp.max(scores, axis=-1))
        exponent = jnp.exp(scores - new_max[..., None])
        factor = jnp.exp(running_max - new_max)
        running_sum = running_sum * factor + jnp.sum(exponent, axis=-1)
        weighted = weighted * factor[..., None] + jnp.einsum(
            "gqn,ngd->gqd",
            exponent.astype(jnp.bfloat16),
            value_block,
            preferred_element_type=jnp.float32,
        )
        return ((new_max, running_sum, weighted), None)

    initial = (
        jnp.full((local_kv, lane_count), -1e30, jnp.float32),
        jnp.zeros((local_kv, lane_count), jnp.float32),
        jnp.zeros((local_kv, lane_count, head_dim), jnp.float32),
    )
    carry = initial
    key_piece, value_piece = sent_together((key_turned, value_rows), "ep", 0, 1)
    piece_rows = key_piece.shape[0]
    block_rows = 512
    block_count = piece_rows // block_rows
    key_split = key_piece.reshape(block_count, block_rows, local_kv, head_dim)
    value_split = value_piece.reshape(block_count, block_rows, local_kv, head_dim)
    carry, _ = lax.scan(attend_block, carry, (key_split, value_split))
    running_max, running_sum, weighted = carry
    attended = (weighted / running_sum[..., None]).astype(jnp.bfloat16)
    attended = (
        attended.reshape(local_kv, group_size, row_count, head_dim)
        .transpose(2, 0, 1, 3)
        .reshape(row_count, local_kv * group_size * head_dim)
    )
    mixed_sum = sum_by_axis(jnp.dot(attended, w_out, preferred_element_type=jnp.float32), TP)
    scaled = (
        mixed_sum
        * lax.rsqrt(jnp.mean(mixed_sum * mixed_sum, axis=1, keepdims=True) + EPS)
        * mixer_gain
    )
    return scaled.astype(jnp.bfloat16)


def expert_half(
    expert_input, expert_ids, expert_weights, input_gain, w_gate, w_up, w_down, out_gain
):
    row_count = expert_input.shape[0]
    top_count = expert_ids.shape[1]
    expert_total = w_gate.shape[0] * lax.axis_size("ep")
    inner_count = expert_total // GROUPS
    capacity = 3 * row_count // (4 * inner_count)
    inputs_f = expert_input.astype(jnp.float32)
    normed = (
        inputs_f
        * lax.rsqrt(jnp.mean(inputs_f * inputs_f, axis=1, keepdims=True) + EPS)
        * input_gain
    ).astype(jnp.bfloat16)
    flat_ids = expert_ids.reshape(-1)
    one_hot = (flat_ids[:, None] == jnp.arange(expert_total, dtype=jnp.int32)[None, :]).astype(
        jnp.int32
    )
    earlier = jnp.cumsum(one_hot, axis=0) - one_hot
    rank_in = jnp.sum(earlier * one_hot, axis=1)
    slot_of = flat_ids * capacity + rank_in
    pick_rows = jnp.arange(flat_ids.shape[0], dtype=jnp.int32) // top_count
    source_row = (
        jnp.full((expert_total * capacity,), row_count, jnp.int32).at[slot_of].set(pick_rows)
    )
    padded = jnp.concatenate([normed, jnp.zeros((1, normed.shape[1]), jnp.bfloat16)], axis=0)
    gate_local = w_gate[0]
    up_local = w_up[0]
    down_local = w_down[0]
    col_width = normed.shape[1] // lax.axis_size(TP)
    col_part = lax.dynamic_slice_in_dim(padded, lax.axis_index(TP) * col_width, col_width, 1)
    outgoing = jnp.take(col_part, source_row, axis=0)
    arrived = lax.all_to_all(outgoing, "ep", split_axis=0, concat_axis=0, tiled=True)
    piece = gathered_copies(arrived, TP, 1)
    gate_pre = jnp.dot(piece, gate_local, preferred_element_type=jnp.float32)
    up_pre = jnp.dot(piece, up_local, preferred_element_type=jnp.float32)
    hidden = (jax.nn.silu(gate_pre) * up_pre).astype(jnp.bfloat16)
    partial_term = jnp.dot(hidden, down_local, preferred_element_type=jnp.float32)
    summed = sent_and_summed(partial_term.astype(jnp.bfloat16), TP, 1).astype(jnp.bfloat16)
    returned = lax.all_to_all(summed, "ep", split_axis=0, concat_axis=0, tiled=True)
    picked = (
        jnp.take(returned, slot_of, axis=0)
        .reshape(row_count, top_count, returned.shape[1])
        .astype(jnp.float32)
    )
    combined = jnp.sum(picked * expert_weights[:, :, None], axis=1)
    squares = taken_together(jnp.sum(combined * combined, axis=1), TP)
    scaled = combined * lax.rsqrt(squares / D + EPS)[:, None] * out_gain
    return scaled.astype(jnp.bfloat16)


def per_device(
    query_rows,
    key_rows,
    value_rows,
    query_gain,
    key_gain,
    w_out,
    mixer_gain,
    expert_input,
    expert_ids,
    expert_weights,
    input_gain,
    w_gate,
    w_up,
    w_down,
    out_gain,
):
    mixer_result = mixer_half(
        query_rows, key_rows, value_rows, query_gain, key_gain, w_out, mixer_gain
    )
    moe_result = expert_half(
        expert_input, expert_ids, expert_weights, input_gain, w_gate, w_up, w_down, out_gain
    )
    return (mixer_result, moe_result)


def solution(mesh):
    finer = Mesh(mesh.devices.reshape(mesh.shape["ep"], 8, 2), ("ep", "tp_0", "tp_1"))
    in_specs = (
        P("ep", TP),
        P("ep", TP),
        P("ep", TP),
        P(),
        P(),
        P(TP, None),
        P(),
        P("ep", None),
        P("ep", None),
        P("ep", None),
        P(),
        P("ep", None, TP),
        P("ep", None, TP),
        P("ep", TP, None),
        P(TP),
    )
    out_specs = (P(EP_TP, None), P("ep", TP))
    return jax.shard_map(
        per_device, mesh=finer, in_specs=in_specs, out_specs=out_specs, check_vma=False
    )
```

profile of v0, /device:TPU:1, one launch (start us, length us, event | category | flops | bytes accessed | tf_op | source)
XLA Modules:
  0.0 286.7 jit_solution(11606591436551511769)
XLA Ops:
  14.8 2.9 %scatter_custom_fusion = s32[576]{0:T(1024)S(1)} fusion(s32[384]{0:T(512)S(1)} %fusion.83, s32[384]{0:T(512)S(1)} %add_select_fusion, s32[]{:T(128)} %constant.145.clone.1), kind=kCustom, calls=%fused_computation.135 | custom fusion | bytes 2308 | tf_op jit(solution)/shard_map/scatter | solution.py:188
  18.4 1.9 gather_fusion
  20.6 24.6 %all_to_all.34 = bf16[32,18,128]{2,1,0:T(8,128)(2,1)S(1)} all-to-all(bf16[32,18,128]{2,1,0:T(8,128)(2,1)S(1)} %broadcast_select_fusion.2), channel_id=1, replica_groups=mesh['ep'=32,'tp_0'=8,'tp_1'=2] {'ep'}, dimensions={0} | all-to-all | bytes 294912 | tf_op jit(solution)/shard_map/all_to_all | solution.py:197
  45.3 1.9 broadcast_in_dim.50
  47.2 10.2 %all-to-all-start.1 = ((bf16[16,576,128]{2,1,0:T(8,128)(2,1)}), bf16[16,576,128]{2,1,0:T(8,128)(2,1)}, u32[]{:S(2)}, u32[]{:S(2)}) async-start(bf16[16,576,128]{2,1,0:T(8,128)(2,1)} %broadcast_in_dim.50), calls=%async_computation.3 | async-start | bytes 4718592 | tf_op jit(solution)/shard_map/all_to_all | solution.py:36
  58.2 1.4 multiply_cosine_fusion.1
  60.1 1.4 fusion.50
  62.8 49.1 %all-to-all-done.1 = bf16[16,576,128]{2,1,0:T(8,128)(2,1)} async-done(((bf16[16,576,128]{2,1,0:T(8,128)(2,1)}), bf16[16,576,128]{2,1,0:T(8,128)(2,1)}, u32[]{:S(2)}, u32[]{:S(2)}) %all-to-all-start.1) | async-done | bytes 2359328 | tf_op jit(solution)/shard_map/all_to_all | solution.py:36
  111.9 2.4 fusion.17
  114.3 6.0 %fusion.21 = bf16[72,16,8,128]{3,2,1,0:T(8,128)(2,1)} fusion(bf16[1,256,2048]{2,1,0:T(8,128)(2,1)S(1)} %copy-done, bf16[1,2048,256]{2,1,0:T(8,128)(2,1)} %param.29, f32[576,256]{1,0:T(8,128)S(1)} %fusion.17, bf16[16,576,128]{2,1,0:T(8,128)(2,1)} %all-to-all-done.1), kind=kOutput, calls=%fused_computation.36 | convolution fusion | flops 1210023936 | bytes 7405568 | tf_op jit(solution)/shard_map/dot_general | solution.py:202
  120.3 3.7 %copy.112 = bf16[72,16,8,128]{3,2,0,1:T(8,128)(2,1)} copy(bf16[72,16,8,128]{3,2,1,0:T(8,128)(2,1)} %fusion.21) | data formatting | bytes 4718592 | tf_op jit(solution)/shard_map/reshape | solution.py:54
  124.0 5.3 %all-to-all-start.2 = ((bf16[16,576,128]{2,1,0:T(8,128)(2,1)}), bf16[16,576,128]{2,1,0:T(8,128)(2,1)}, u32[]{:S(2)}, u32[]{:S(2)}) async-start(bf16[16,576,128]{2,1,0:T(8,128)(2,1)} %bitcast.113), calls=%async_computation.4 | async-start | bytes 4718592 | tf_op jit(solution)/shard_map/all_to_all | solution.py:60
  129.3 6.2 %fusion.87 = (bf16[12288,128]{0,1:T(8,128)(2,1)}, bf16[12288,128]{0,1:T(8,128)(2,1)}) fusion(bf16[12288,256]{0,1:T(8,128)(2,1)} %all-gather.2.cloned.1.call-done), kind=kLoop, calls=%fused_computation.152 | loop fusion | bytes 12582912 | tf_op jit(solution)/shard_map/split | solution.py:24
  135.5 4.6 %copy.77 = bf16[12288,128]{1,0:T(8,128)(2,1)} copy(bf16[12288,128]{0,1:T(8,128)(2,1)} %get-tuple-element.127) | data formatting | bytes 6291456 | tf_op jit(solution)/shard_map/split | solution.py:24
  140.1 4.7 %copy.73 = bf16[12288,128]{1,0:T(8,128)(2,1)} copy(bf16[12288,128]{0,1:T(8,128)(2,1)} %get-tuple-element.128) | data formatting | bytes 6291456 | tf_op jit(solution)/shard_map/split | solution.py:24
  144.8 73.8 %while.15 = (s32[]{:T(128)}, f32[1,768]{1,0:T(1,128)S(1)}, f32[1,768]{1,0:T(1,128)S(1)}, f32[1,768,128]{2,1,0:T(8,128)S(1)}, bf16[24,512,1,128]{3,1,2,0:T(8,128)...) while((s32[]{:T(128)}, f32[1,768]{1,0:T(1,128)S(1)}, ...), condition=%wide.region_5.6_spmd.clone, body=%wide.region_2.5_spmd.clone.sunk | while | flops 203985408 | bytes 6016121 | solution.py:148
  146.5 1.4 fusion.105
  149.6 1.4 fusion.105
  152.7 1.4 fusion.105
  155.7 1.4 fusion.105
  158.8 1.4 fusion.105
  161.9 1.4 fusion.105
  164.9 1.4 fusion.105
  168.0 1.4 fusion.105
  171.1 1.4 fusion.105
  174.2 1.4 fusion.105
  177.2 1.4 fusion.105
  180.3 1.4 fusion.105
  183.4 1.4 fusion.105
  186.5 1.4 fusion.105
  189.5 1.4 fusion.105
  192.6 1.4 fusion.105
  195.7 1.4 fusion.105
  198.8 1.4 fusion.105
  201.8 1.4 fusion.105
  204.9 1.4 fusion.105
  208.0 1.4 fusion.105
  211.1 1.4 fusion.105
  214.1 1.4 fusion.105
  217.2 1.4 fusion.105
  219.1 1.8 convolution_convert_fusion.1
  221.1 2.0 reduce_sum.106
  223.8 3.9 %all-to-all-start.3 = ((bf16[32,18,128]{2,1,0:T(8,128)(2,1)}), bf16[32,18,128]{2,1,0:T(8,128)(2,1)S(1)}, u32[]{:S(2)}, u32[]{:S(2)}) async-start(bf16[32,18,128]{2,1,0:T(8,128)(2,1)} %all_to_all.25), calls=%async_computation.5 | async-start | bytes 393216 | tf_op jit(solution)/shard_map/all_to_all | solution.py:204
  228.1 10.3 %all-to-all-done.3 = bf16[32,18,128]{2,1,0:T(8,128)(2,1)S(1)} async-done(((bf16[32,18,128]{2,1,0:T(8,128)(2,1)}), bf16[32,18,128]{2,1,0:T(8,128)(2,1)S(1)}, u32[]{:S(2)}, u32[]{:S(2)}) %all-to-all-start.3) | async-done | bytes 147488 | tf_op jit(solution)/shard_map/all_to_all | solution.py:204
  238.4 1.4 gather_fusion.1
  241.1 16.0 %all_to_all.35 = f32[16,1,192]{2,1,0:T(1,128)S(1)} all-to-all(f32[16,1,192]{2,1,0:T(1,128)S(1)} %broadcast_in_dim.87), channel_id=1, replica_groups=mesh['ep'=32,'tp_0'=8,'tp_1'=2] {'tp_0','tp_1'}, dimensions={0} | all-to-all | bytes 24576 | tf_op jit(solution)/shard_map/all_to_all | solution.py:36
  258.0 19.5 %reduce-scatter.5.cloned.1.call-done = bf16[24,2048]{1,0:T(8,128)(2,1)} async-done(((bf16[48,2048]{1,0:T(8,128)(2,1)}), bf16[24,2048]{1,0:T(8,128)(2,1)}) %reduce-scatter.5.cloned.1.call-update) | async-done | bytes 98320 | tf_op jit(solution)/shard_map/reduce_scatter | solution.py:30
  278.5 1.6 fusion.49
  (213 shorter events, 53.9 us)
Async XLA Ops:
  7.2 107.1 %copy-start = (bf16[1,256,2048]{2,1,0:T(8,128)(2,1)S(1)}, bf16[1,256,2048]{2,1,0:T(8,128)(2,1)}, u32[]{:S(2)}) copy-start(bf16[1,256,2048]{2,1,0:T(8,128)(2,1)} %param.30) | copy-start | bytes 3145732
  7.2 10.7 %copy-start.1 = (bf16[192,2048]{1,0:T(8,128)(2,1)S(1)}, bf16[192,2048]{1,0:T(8,128)(2,1)}, u32[]{:S(2)}) copy-start(bf16[192,2048]{1,0:T(8,128)(2,1)} %param.24) | copy-start | bytes 2359300
  7.2 10.9 %copy-start.5 = (f32[2048]{0:T(1024)S(1)}, f32[2048]{0:T(1024)}, u32[]{:S(2)}) copy-start(f32[2048]{0:T(1024)} %param.27) | copy-start | bytes 24580
  7.2 122.1 %all-gather.2.cloned.1.call-start = ((), (), s32[]{:S(2)}) async-start(), calls=%async_computation.7 | async-start | bytes 6488064 | tf_op jit(solution)/shard_map/all_gather | solution.py:24
  47.2 10.3 %copy-start.3 = (bf16[384,256]{1,0:T(8,128)(2,1)S(1)}, bf16[384,256]{1,0:T(8,128)(2,1)}, u32[]{:S(2)}) copy-start(bf16[384,256]{1,0:T(8,128)(2,1)} %param.17) | copy-start | bytes 589828
  47.2 64.7 %all-to-all-start.1 = ((bf16[16,576,128]{2,1,0:T(8,128)(2,1)}), bf16[16,576,128]{2,1,0:T(8,128)(2,1)}, u32[]{:S(2)}, u32[]{:S(2)}) async-start(bf16[16,576,128]{2,1,0:T(8,128)(2,1)} %broadcast_in_dim.50), calls=%async_computation.3 | async-start | bytes 4718592 | tf_op jit(solution)/shard_map/all_to_all | solution.py:36
  57.4 2.2 copy-start.8
  60.1 51.7 %copy-start.10 = (bf16[1,2048,256]{2,1,0:T(8,128)(2,1)S(1)}, bf16[1,2048,256]{2,1,0:T(8,128)(2,1)}, u32[]{:S(2)}) copy-start(bf16[1,2048,256]{2,1,0:T(8,128)(2,1)} %param.28) | copy-start | bytes 3145732
  124.0 97.1 %all-to-all-start.2 = ((bf16[16,576,128]{2,1,0:T(8,128)(2,1)}), bf16[16,576,128]{2,1,0:T(8,128)(2,1)}, u32[]{:S(2)}, u32[]{:S(2)}) async-start(bf16[16,576,128]{2,1,0:T(8,128)(2,1)} %bitcast.113), calls=%async_computation.4 | async-start | bytes 4718592 | tf_op jit(solution)/shard_map/all_to_all | solution.py:60
  129.3 128.0 %reduce-scatter.3.cloned.1.call-start = ((), (), s32[]{:S(2)}) async-start(), calls=%async_computation.8 | async-start | bytes 1769472 | tf_op jit(solution)/shard_map/reduce_scatter | solution.py:30
  144.8 74.2 %copy-start.2 = (bf16[256,2048]{1,0:T(8,128)(2,1)S(1)}, bf16[256,2048]{1,0:T(8,128)(2,1)}, u32[]{:S(2)}) copy-start(bf16[256,2048]{1,0:T(8,128)(2,1)} %param.22) | copy-start | bytes 3145732
  220.8 6.9 %copy-start.4 = (s32[192,2]{0,1:T(2,128)S(1)}, s32[192,2]{0,1:T(2,128)}, u32[]{:S(2)}) copy-start(s32[192,2]{0,1:T(2,128)} %param.25) | copy-start | bytes 4612
  220.8 7.1 %copy-start.7 = (f32[192,2]{0,1:T(2,128)S(1)}, f32[192,2]{0,1:T(2,128)}, u32[]{:S(2)}) copy-start(f32[192,2]{0,1:T(2,128)} %param.26) | copy-start | bytes 4612
  221.1 36.2 %copy-start.9 = (f32[128]{0:T(128)S(1)}, f32[128]{0:T(128)}, u32[]{:S(2)}) copy-start(f32[128]{0:T(128)} %param.31) | copy-start | bytes 1540
  221.1 57.4 %copy-start.6 = (f32[2048]{0:T(1024)S(1)}, f32[2048]{0:T(1024)}, u32[]{:S(2)}) copy-start(f32[2048]{0:T(1024)} %param.23) | copy-start | bytes 24580
  223.8 14.5 %all-to-all-start.3 = ((bf16[32,18,128]{2,1,0:T(8,128)(2,1)}), bf16[32,18,128]{2,1,0:T(8,128)(2,1)S(1)}, u32[]{:S(2)}, u32[]{:S(2)}) async-start(bf16[32,18,128]{2,1,0:T(8,128)(2,1)} %all_to_all.25), calls=%async_computation.5 | async-start | bytes 393216 | tf_op jit(solution)/shard_map/all_to_all | solution.py:204
  227.7 49.8 %reduce-scatter.5.cloned.1.call-start = ((), (), s32[]{:S(2)}) async-start(), calls=%async_computation.9 | async-start | bytes 294912 | tf_op jit(solution)/shard_map/reduce_scatter | solution.py:30
Sparse Core Ops, SparseCore 0:
  11.6 101.6 all-gather.1
  221.0 33.1 reduce-scatter.2
  257.4 20.0 reduce-scatter.4
where the time goes:
time: 288 us; the launch traced here: 287 us
  waiting for transfers between devices  78.9 us (27%)
  matrix products  75.5 us (26%)
  blocking collectives  40.6 us (14%)
  local copies, waits for them, and re-layouts  33.1 us (11%)
  other arithmetic  23.6 us (8%)
  starting transfers between devices  19.5 us (7%)
  between operations  14.2 us (5%)
    all_to_all x1, waiting for transfers between devices, sent_to_all(): lax.all_to_all(jnp.broadcast_to(shard[None], (count, *shard.shape)), axis...  49.1 us
    dot_general x24, matrix products, attend_block(): jnp.einsum('gqn,ngd->gqd', exponent.astype(jnp.bfloat16), value_block, pr...  34.5 us
    dot_general x24, matrix products, attend_block(): jnp.einsum('gqd,ngd->gqn', grouped, key_block, preferred_element_type=jnp...  30.8 us
    all_to_all x1, blocking collectives, expert_half(): lax.all_to_all(outgoing, 'ep', split_axis=0, concat_axis=0, tiled=True)  24.6 us
    reduce_scatter x2, waiting for transfers between devices, sum_by_axis(): running = lax.psum_scatter(running, axis, scatter_dimension=0, tiled=True)  19.5 us
    all_to_all x1, blocking collectives, sent_to_all(): lax.all_to_all(jnp.broadcast_to(shard[None], (count, *shard.shape)), axis...  16 us
    split x3, local copies, waits for them, and re-layouts, sent_together(): jnp.split(lax.all_gather(both, axis, axis=dim, tiled=True), ends, axis=al...  15.5 us
    all_to_all x1, waiting for transfers between devices, expert_half(): lax.all_to_all(summed, 'ep', split_axis=0, concat_axis=0, tiled=True)  10.3 us
  transfers between devices with their start and end apart: 6, of which 3 were waited for; matrix products, arithmetic and copies ran while one was open for 43% of the time, Pallas kernels for 0%

commit v1 on v0

v1 whole, which is shorter than its diff:
```python
import functools
from types import SimpleNamespace

import numpy as np
import jax
import jax.numpy as jnp
from jax import lax
from jax.experimental import pallas as pl
from jax.experimental.pallas import tpu as pltpu
from jax.sharding import Mesh
from jax.sharding import PartitionSpec as P

NZ, NX, NY, NC = 8, 4, 8, 2
EP = ("z", "x")
TP = ("y", "c")
D = 2048
HEAD = 128
GRID = 64
ROWS = 384
TOKENS2 = 192
CAP = 18
SLAB = 32
EXPERTS = 32
SLOTS = EXPERTS * CAP
PADDED = EXPERTS * SLAB
EPS = 1e-06
THETA = 10000.0
F32 = jnp.float32
BF16 = jnp.bfloat16
MESH_ID = pl.DeviceIdType.MESH
FAR_FIRST = (4, 3, 5, 2, 6, 1, 7, 0)
X_ORDER = (2, 1, 3, 0)


def around(i, d, n):
    return lax.rem(i + (d % n), n)


def here():
    a = SimpleNamespace()
    a.z, a.x, a.y, a.c = (lax.axis_index(n) for n in ("z", "x", "y", "c"))
    a.ep = a.z * NX + a.x
    return a


def remote(src, dst, ss, rs, **dev):
    return pltpu.make_async_remote_copy(
        src_ref=src, dst_ref=dst, send_sem=ss, recv_sem=rs, device_id=dev, device_id_type=MESH_ID
    )


def ep_peer(a, k):
    e = lax.rem(a.ep + k, EXPERTS)
    return e, lax.div(e, NX), lax.rem(e, NX)


def greet_ep(a, barrier):
    def one(k, carry):
        _, z, x = ep_peer(a, k)
        pl.semaphore_signal(barrier, inc=1, device_id={"z": z, "x": x}, device_id_type=MESH_ID)
        return carry

    lax.fori_loop(1, EXPERTS, one, 0)


def greet_tp(a, barrier, cores):
    for d in range(NY):
        for o in range(cores):
            if d or o:
                c = a.c if o == 0 else 1 - a.c
                pl.semaphore_signal(
                    barrier, inc=1, device_id={"y": around(a.y, d, NY), "c": c}, device_id_type=MESH_ID
                )


def wait_bytes(ref, sem):
    pltpu.make_async_copy(ref, ref, sem).wait()


def iota(shape, dim):
    return lax.broadcasted_iota(jnp.int32, shape, dim)


def eye128():
    return iota((128, 128), 0) == iota((128, 128), 1)


def to_row(col):
    return jnp.sum(jnp.where(eye128(), col, 0.0), axis=0, keepdims=True)


def to_col(row):
    return jnp.sum(jnp.where(eye128(), row, 0.0), axis=1, keepdims=True)


MOE_IN = ("xin", "srow", "scol", "wts", "igain", "ogain", "wg_h", "wu_h", "wd_h")
MOE_SCRATCH = dict(
    disp=pltpu.VMEM((EXPERTS, SLAB, 256), BF16),
    drecv=pltpu.VMEM((EXPERTS, SLAB, 256), BF16),
    xg=pltpu.VMEM((2, 4, 2, SLOTS, 128), BF16),
    xcat=pltpu.VMEM((SLOTS, D), BF16),
    wg=pltpu.VMEM((D, 256), BF16),
    wu=pltpu.VMEM((D, 256), BF16),
    wd=pltpu.VMEM((256, D), BF16),
    part=pltpu.VMEM((2, NY, SLOTS, 128), BF16),
    pr=pltpu.VMEM((NY, SLOTS, 128), BF16),
    ps=pltpu.VMEM((NY, SLOTS, 128), BF16),
    own=pltpu.VMEM((SLOTS, 128), F32),
    rs=pltpu.VMEM((NY, SLOTS, 128), BF16),
    rsend=pltpu.VMEM((EXPERTS, SLAB, 128), BF16),
    rrecv=pltpu.VMEM((EXPERTS, SLAB, 128), BF16),
    comb=pltpu.VMEM((TOKENS2, 128), F32),
    sqs=pltpu.VMEM((8, 128), F32),
    sqr=pltpu.VMEM((16, 8, 128), F32),
    w_sem=pltpu.SemaphoreType.DMA((3,)),
    d_ss=pltpu.SemaphoreType.DMA,
    d_rs=pltpu.SemaphoreType.DMA,
    ag_ss=pltpu.SemaphoreType.DMA((3,)),
    ag_rs=pltpu.SemaphoreType.DMA((3,)),
    pf_ss=pltpu.SemaphoreType.DMA((4,)),
    pf_rs=pltpu.SemaphoreType.DMA((4,)),
    pp_ss=pltpu.SemaphoreType.DMA((8,)),
    pp_rs=pltpu.SemaphoreType.DMA((8,)),
    rs_ss=pltpu.SemaphoreType.DMA((8,)),
    rs_rs=pltpu.SemaphoreType.DMA((8,)),
    t_ss=pltpu.SemaphoreType.DMA,
    t_rs=pltpu.SemaphoreType.DMA,
    q_ss=pltpu.SemaphoreType.DMA,
    q_rs=pltpu.SemaphoreType.DMA,
)


def moe_weights(r):
    for i, (src, dst) in enumerate(((r.wg_h, r.wg), (r.wu_h, r.wu), (r.wd_h, r.wd))):
        pltpu.make_async_copy(src, dst, r.w_sem.at[i]).start()


def moe_weights_wait(r):
    for i, (src, dst) in enumerate(((r.wg_h, r.wg), (r.wu_h, r.wu), (r.wd_h, r.wd))):
        pltpu.make_async_copy(src, dst, r.w_sem.at[i]).wait()


def moe_dispatch_build(a, r):
    x = r.xin[...].astype(F32)
    inv = lax.rsqrt(jnp.sum(x * x, axis=1, keepdims=True) * (1.0 / D) + EPS)
    g = lax.rem(a.y, 4)
    halves = []
    for j in range(2):
        off = pl.multiple_of(((g + 4 * j) * 2 + a.c) * 128, 128)
        xs = r.xin[:, pl.ds(off, 128)].astype(F32)
        halves.append((xs * inv * r.igain[:, pl.ds(off, 128)]).astype(BF16))
    nn = jnp.concatenate(halves, axis=1)
    rows = iota((PADDED, TOKENS2), 0)
    pick = (rows == r.srow[0:1, :]) | (rows == r.srow[1:2, :])
    pick = jnp.where(pick, 1.0, 0.0).astype(BF16)
    out = jnp.dot(pick, nn, preferred_element_type=F32).astype(BF16)
    r.disp[...] = out.reshape(EXPERTS, SLAB, 256)


def exchange_start(a, src, dst, ss, rs):
    def one(k, carry):
        e, z, x = ep_peer(a, k)
        remote(src.at[e], dst.at[a.ep], ss, rs, z=z, x=x).start()
        return carry

    lax.fori_loop(1, EXPERTS, one, 0)
    dst[a.ep] = src[a.ep]


def exchange_wait(src, dst, ss, rs):
    wait_bytes(dst.at[pl.ds(0, EXPERTS - 1)], rs)
    wait_bytes(src.at[pl.ds(0, EXPERTS - 1)], ss)


def padded_place(i):
    e = ((i.astype(F32) + 0.5) * (1.0 / CAP)).astype(jnp.int32)
    return i + e * (SLAB - CAP)


def moe_compact(a, r):
    g = lax.rem(a.y, 4)
    place = padded_place(iota((SLOTS, 1), 0))
    pick = jnp.where(iota((SLOTS, PADDED), 1) == place, 1.0, 0.0).astype(BF16)
    got = r.drecv[...].reshape(PADDED, 256)
    out = jnp.dot(pick, got, preferred_element_type=F32).astype(BF16)
    r.xg[a.c, g, 0] = out[:, :128]
    r.xg[a.c, g, 1] = out[:, 128:]


def moe_gather_copies(a, r):
    g = lax.rem(a.y, 4)
    src = r.xg.at[a.c, g]
    two = around(a.y, 2, NY) + a.c * 4
    targets = (around(a.y, 1, NY), around(a.y, -1, NY), lax.rem(two, NY))
    return [remote(src, src, r.ag_ss.at[i], r.ag_rs.at[i], y=t) for i, t in enumerate(targets)]


def moe_group(a, i):
    g = lax.rem(a.y, 4)
    return g if i == 0 else around(g, (3, 1, 2)[i - 1], 4)


def moe_partner_copy(a, r, i):
    src = r.xg.at[a.c, moe_group(a, i)]
    return remote(src, src, r.pf_ss.at[i], r.pf_rs.at[i], c=1 - a.c)


def moe_gather_start(a, r):
    for cp in moe_gather_copies(a, r):
        cp.start()
    moe_partner_copy(a, r, 0).start()


def moe_gather_forward(a, r, i):
    moe_gather_copies(a, r)[i - 1].wait_recv()
    moe_partner_copy(a, r, i).start()


def moe_gather_finish(a, r):
    for cp in moe_gather_copies(a, r):
        cp.wait_send()
    for i in range(4):
        moe_partner_copy(a, r, i).wait()


def moe_experts(a, r):
    for par in range(2):
        for g in range(4):
            for h in range(2):
                at = ((g + 4 * h) * 2 + par) * 128
                r.xcat[:, at : at + 128] = r.xg[par, g, h]
    moe_weights_wait(r)

    def block(b, carry):
        at = pl.ds(pl.multiple_of(b * 192, 192), 192)
        xb = r.xcat[at, :]
        gate = jnp.dot(xb, r.wg[...], preferred_element_type=F32)
        up = jnp.dot(xb, r.wu[...], preferred_element_type=F32)
        hid = (gate / (1.0 + jnp.exp(-gate)) * up).astype(BF16)
        for ys in range(NY):
            o = jnp.dot(hid, r.wd[:, ys * 256 : ys * 256 + 256], preferred_element_type=F32)
            o = o.astype(BF16)
            r.part[0, ys, at, :] = o[:, :128]
            r.part[1, ys, at, :] = o[:, 128:]
        return carry

    lax.fori_loop(0, SLOTS // 192, block, 0)


def moe_pair_copy(a, r, i):
    ys = around(a.y, FAR_FIRST[i], NY)
    return remote(r.part.at[1 - a.c, ys], r.pr.at[ys], r.pp_ss.at[i], r.pp_rs.at[i], c=1 - a.c)


def moe_sum_copy(a, r, d):
    ys = around(a.y, d, NY)
    return remote(r.ps.at[ys], r.rs.at[d], r.rs_ss.at[d], r.rs_rs.at[d], y=ys)


def moe_pair_start(a, r):
    for i in range(NY):
        moe_pair_copy(a, r, i).start()


def moe_pair_sum(a, r, i):
    d = FAR_FIRST[i]
    ys = around(a.y, d, NY)
    moe_pair_copy(a, r, i).wait_recv()
    total = r.part[a.c, ys].astype(F32) + r.pr[ys].astype(F32)
    if d:
        r.ps[ys] = total.astype(BF16)
        moe_sum_copy(a, r, d).start()
    else:
        r.own[...] = total


def moe_return_start(a, r):
    total = r.own[...]
    for d in range(1, NY):
        moe_sum_copy(a, r, d).wait_recv()
        total = total + r.rs[d].astype(F32)
    rows = total.astype(BF16)
    place = padded_place(iota((1, SLOTS), 1))
    pick = jnp.where(iota((PADDED, SLOTS), 0) == place, 1.0, 0.0).astype(BF16)
    out = jnp.dot(pick, rows, preferred_element_type=F32).astype(BF16)
    r.rsend[...] = out.reshape(EXPERTS, SLAB, 128)
    exchange_start(a, r.rsend, r.rrecv, r.t_ss, r.t_rs)


def square_targets(a):
    out = []
    for d in range(NY):
        for o in range(2):
            if d or o:
                out.append((around(a.y, d, NY), a.c if o == 0 else 1 - a.c))
    return out


def moe_combine(a, r):
    exchange_wait(r.rsend, r.rrecv, r.t_ss, r.t_rs)
    got = r.rrecv[...].reshape(PADDED, 128)
    total = None
    for k in range(2):
        pick = jnp.where(iota((TOKENS2, PADDED), 1) == r.scol[:, k : k + 1], 1.0, 0.0).astype(BF16)
        term = jnp.dot(pick, got, preferred_element_type=F32) * r.wts[:, k : k + 1]
        total = term if total is None else total + term
    r.comb[...] = total
    sq = jnp.sum(total * total, axis=1, keepdims=True)
    r.sqs[...] = jnp.zeros((8, 128), F32)
    r.sqs[0:1, :] = to_row(sq[:128])
    r.sqs[1:2, :] = to_row(sq[64:])
    tp = a.y * 2 + a.c
    for y, c in square_targets(a):
        remote(r.sqs, r.sqr.at[tp], r.q_ss, r.q_rs, y=y, c=c).start()
    r.sqr[tp] = r.sqs[...]


def moe_finish(a, r, out):
    wait_bytes(r.sqr.at[pl.ds(0, 15)], r.q_rs)
    wait_bytes(r.sqr.at[pl.ds(0, 15)], r.q_ss)
    tot = r.sqr[0]
    for i in range(1, 16):
        tot = tot + r.sqr[i]
    inv = lax.rsqrt(tot * (1.0 / D) + EPS)
    lo, hi = to_col(inv[0:1, :]), to_col(inv[1:2, :])
    out[0:128, :] = (r.comb[0:128, :] * lo * r.ogain[...]).astype(BF16)
    out[128:192, :] = (r.comb[128:192, :] * hi[64:] * r.ogain[...]).astype(BF16)
    for d in range(1, NY):
        moe_sum_copy(a, r, d).wait_send()
    for i in range(NY):
        moe_pair_copy(a, r, i).wait_send()


MIX_IN = ("q_in", "k_in", "v_in", "qg", "kg", "rowcs", "colcs", "mgain", "wo_h")
MIX_SCRATCH = dict(
    q_all=pltpu.VMEM((NX, 2 * ROWS, HEAD), BF16),
    kt=pltpu.VMEM((NZ, HEAD, ROWS), BF16),
    va=pltpu.VMEM((NZ, ROWS, HEAD), BF16),
    kx=pltpu.VMEM((HEAD, 2 * ROWS), BF16),
    vx=pltpu.VMEM((2 * ROWS, 256), BF16),
    mx=pltpu.VMEM((NX, 2 * ROWS, 128), F32),
    acc=pltpu.VMEM((NX, 2 * ROWS, 256), F32),
    ob=pltpu.VMEM((NX, 2 * ROWS, HEAD), BF16),
    lb=pltpu.VMEM((NX, 8, 128), F32),
    orc=pltpu.VMEM((NX, 2 * ROWS, HEAD), BF16),
    lrc=pltpu.VMEM((NX, 8, 128), F32),
    att=pltpu.VMEM((ROWS, 256), BF16),
    wo=pltpu.VMEM((256, D), BF16),
    mp=pltpu.VMEM((2, ROWS, 1024), BF16),
    mr=pltpu.VMEM((ROWS, 1024), BF16),
    ms=pltpu.VMEM((NY, 48, 1024), BF16),
    yr=pltpu.VMEM((NY, 48, 1024), BF16),
    fs=pltpu.VMEM((48, 1024), F32),
    fr=pltpu.VMEM((24, 1024), F32),
    wo_sem=pltpu.SemaphoreType.DMA,
    xq_ss=pltpu.SemaphoreType.DMA((4,)),
    xq_rs=pltpu.SemaphoreType.DMA((4,)),
    k_ss=pltpu.SemaphoreType.DMA((8,)),
    k_rs=pltpu.SemaphoreType.DMA((8,)),
    v_ss=pltpu.SemaphoreType.DMA((8,)),
    v_rs=pltpu.SemaphoreType.DMA((8,)),
    o_ss=pltpu.SemaphoreType.DMA((4,)),
    o_rs=pltpu.SemaphoreType.DMA((4,)),
    l_ss=pltpu.SemaphoreType.DMA((4,)),
    l_rs=pltpu.SemaphoreType.DMA((4,)),
    m_ss=pltpu.SemaphoreType.DMA((2,)),
    m_rs=pltpu.SemaphoreType.DMA((2,)),
    y_ss=pltpu.SemaphoreType.DMA((8,)),
    y_rs=pltpu.SemaphoreType.DMA((8,)),
    f_ss=pltpu.SemaphoreType.DMA,
    f_rs=pltpu.SemaphoreType.DMA,
)
OWN = 7


def swap_parts(v):
    lane = lax.rem(iota(v.shape, 1), 64)
    return jnp.where(lane < 32, pltpu.roll(v, 96, 1), pltpu.roll(v, 32, 1))


def turned(a, r, block, gain, g):
    v = block.astype(F32)
    v = v * lax.rsqrt(jnp.mean(v * v, axis=1, keepdims=True) + EPS) * gain
    at = a.ep * (ROWS // GRID) + g
    cos = r.rowcs[0, pl.ds(at, 1), :] + r.colcs[0]
    sin = r.rowcs[1, pl.ds(at, 1), :] + r.colcs[1]
    return (v * cos + swap_parts(v) * sin).astype(BF16)


def mix_turn(a, r):
    pltpu.make_async_copy(r.wo_h, r.wo, r.wo_sem).start()
    keys = []
    for g in range(ROWS // GRID):
        at = slice(g * GRID, g * GRID + GRID)
        for h in range(2):
            q = turned(a, r, r.q_in[at, h * 128 : h * 128 + 128], r.qg[...], g)
            r.q_all[a.x, h * ROWS + g * GRID : h * ROWS + g * GRID + GRID, :] = q
        keys.append(turned(a, r, r.k_in[at, :], r.kg[...], g))
    key = jnp.concatenate(keys, axis=0)
    r.kt[OWN] = key.astype(F32).T.astype(BF16)
    r.va[OWN] = r.v_in[...]
    r.vx[:, 128:] = jnp.ones((2 * ROWS, 128), BF16)
    r.mx[...] = jnp.full(r.mx.shape, -1e30, F32)
    r.acc[...] = jnp.zeros(r.acc.shape, F32)


def q_copy(a, r, d):
    mine = r.q_all.at[a.x]
    return remote(mine, mine, r.xq_ss.at[d], r.xq_rs.at[d], x=around(a.x, d, NX))


def kv_copies(a, r, slot):
    src = OWN if slot < 2 else slot - 2
    z = around(a.z, 1 if slot % 2 == 0 else -1, NZ)
    return (
        remote(r.kt.at[src], r.kt.at[slot], r.k_ss.at[slot], r.k_rs.at[slot], z=z),
        remote(r.va.at[src], r.va.at[slot], r.v_ss.at[slot], r.v_rs.at[slot], z=z),
    )


def kv_start(a, r, slot):
    for cp in kv_copies(a, r, slot):
        cp.start()


def kv_arrived(a, r, slot):
    for cp in kv_copies(a, r, slot):
        cp.wait_recv()
    if slot + 2 < OWN:
        kv_start(a, r, slot + 2)


def mix_send(a, r):
    kv_start(a, r, 0)
    kv_start(a, r, 1)
    for d in (2, 1, 3):
        q_copy(a, r, d).start()


def attend_rows(r, xs, at):
    q = r.q_all[xs, at, :]
    s = jnp.dot(q, r.kx[...], preferred_element_type=F32)
    old = r.mx[xs, at, :]
    new = jnp.maximum(old, jnp.max(s, axis=1, keepdims=True))
    r.mx[xs, at, :] = new
    p = jnp.concatenate(
        [jnp.exp2(s[:, j * 128 : j * 128 + 128] - new).astype(BF16) for j in range(6)], axis=1
    )
    keep = jnp.exp2(old - new)
    pv = jnp.dot(p, r.vx[...], preferred_element_type=F32)
    acc = r.acc[xs, at, :]
    r.acc[xs, at, :] = acc * jnp.concatenate([keep, keep], axis=1) + pv


TILE = 256


def mix_step(a, r, s):
    slots = (2 * s, 2 * s + 1)
    for slot in slots:
        if slot != OWN:
            kv_arrived(a, r, slot)
    for i, slot in enumerate(slots):
        r.kx[:, i * ROWS : i * ROWS + ROWS] = r.kt[slot]
        r.vx[i * ROWS : i * ROWS + ROWS, :128] = r.va[slot]


def mix_all_rows(a, r):
    def one(xs, carry):
        for t in range(2 * ROWS // TILE):
            attend_rows(r, xs, slice(t * TILE, t * TILE + TILE))
        return carry

    lax.fori_loop(0, NX, one, 0)


def part_copies(a, r, d):
    x = around(a.x, d, NX)
    return (
        remote(r.ob.at[d], r.orc.at[d], r.o_ss.at[d], r.o_rs.at[d], x=x),
        remote(r.lb.at[d], r.lrc.at[d], r.l_ss.at[d], r.l_rs.at[d], x=x),
    )


def mix_last_rows(a, r):
    for d in X_ORDER:
        xs = around(a.x, d, NX)
        dst_o, dst_l = (r.ob, r.lb) if d else (r.orc, r.lrc)
        for t in range(2 * ROWS // TILE):
            at = slice(t * TILE, t * TILE + TILE)
            attend_rows(r, xs, at)
            acc = r.acc[xs, at, :]
            total = acc[:, 128:]
            dst_o[d, at, :] = (acc[:, :128] / total).astype(BF16)
            lse = r.mx[xs, at, :] + jnp.log2(total)
            for b in range(TILE // 128):
                row = t * (TILE // 128) + b
                dst_l[d, row : row + 1, :] = to_row(lse[b * 128 : b * 128 + 128, :])
        if d:
            for cp in part_copies(a, r, d):
                cp.start()


def mix_combine(a, r):
    for d in (1, 2, 3):
        for cp in part_copies(a, r, d):
            cp.wait_recv()
    for b in range(6):
        lse = [to_col(r.lrc[d, b : b + 1, :]) for d in range(NX)]
        top = functools.reduce(jnp.maximum, lse)
        w = [jnp.exp2(v - top) for v in lse]
        inv = 1.0 / functools.reduce(jnp.add, w)
        at = slice(b * 128, b * 128 + 128)
        o = None
        for d in range(NX):
            term = r.orc[d, at, :].astype(F32) * (w[d] * inv)
            o = term if o is None else o + term
        h, t = b // 3, b % 3
        r.att[t * 128 : t * 128 + 128, h * 128 : h * 128 + 128] = o.astype(BF16)


def project(r, half):
    for j in range(4):
        off = pl.multiple_of(half * 1024 + j * 256, 256)
        o = jnp.dot(r.att[...], r.wo[:, pl.ds(off, 256)], preferred_element_type=F32)
        r.mp[half, :, j * 256 : j * 256 + 256] = o.astype(BF16)


def mix_pair_copy(a, r):
    return remote(r.mp.at[1 - a.c], r.mr, r.m_ss.at[0], r.m_rs.at[0], c=1 - a.c)


def mix_sum_copy(a, r, d):
    y = around(a.y, d, NY)
    return remote(r.ms.at[y], r.yr.at[d], r.y_ss.at[d], r.y_rs.at[d], y=y)


def mix_project(a, r):
    pltpu.make_async_copy(r.wo_h, r.wo, r.wo_sem).wait()
    project(r, 1 - a.c)
    mix_pair_copy(a, r).start()
    project(r, a.c)
    mix_pair_copy(a, r).wait_recv()


def mix_scatter(a, r):
    for d in FAR_FIRST:
        y = around(a.y, d, NY)
        at = pl.ds(pl.multiple_of(y * 48, 16), 48)
        total = r.mp[a.c, at, :].astype(F32) + r.mr[at, :].astype(F32)
        if d:
            r.ms[y] = total.astype(BF16)
            mix_sum_copy(a, r, d).start()
        else:
            r.fs[...] = total


def mix_final_copy(a, r):
    src = r.fs.at[pl.ds(pl.multiple_of((1 - a.c) * 24, 8), 24)]
    return remote(src, r.fr, r.f_ss, r.f_rs, c=1 - a.c)


def mix_sum(a, r):
    total = r.fs[...]
    for d in range(1, NY):
        mix_sum_copy(a, r, d).wait_recv()
        total = total + r.yr[d].astype(F32)
    r.fs[...] = total
    mix_final_copy(a, r).start()


def mix_finish(a, r, out):
    mix_final_copy(a, r).wait()
    mine = r.fs[pl.ds(pl.multiple_of(a.c * 24, 8), 24), :]
    other = r.fr[...]
    sq = jnp.sum(mine * mine, axis=1, keepdims=True) + jnp.sum(other * other, axis=1, keepdims=True)
    inv = lax.rsqrt(sq * (1.0 / D) + EPS)
    for half, v in ((a.c, mine), (1 - a.c, other)):
        off = pl.ds(pl.multiple_of(half * 1024, 1024), 1024)
        out[:, off] = (v * inv * r.mgain[:, off]).astype(BF16)
    for d in (1, 2, 3):
        q_copy(a, r, d).wait_send()
        for cp in part_copies(a, r, d):
            cp.wait_send()
    for slot in range(OWN):
        for cp in kv_copies(a, r, slot):
            cp.wait_send()
    mix_pair_copy(a, r).wait_send()
    for d in range(1, NY):
        mix_sum_copy(a, r, d).wait_send()


def bind(names, refs):
    return SimpleNamespace(**dict(zip(names, refs, strict=True)))


def moe_kernel(*refs):
    r = bind((*MOE_IN, "out", *MOE_SCRATCH), refs)
    a = here()
    barrier = pltpu.get_barrier_semaphore()
    greet_ep(a, barrier)
    greet_tp(a, barrier, 2)
    moe_weights(r)
    moe_dispatch_build(a, r)
    pl.semaphore_wait(barrier, 46)
    exchange_start(a, r.disp, r.drecv, r.d_ss, r.d_rs)
    exchange_wait(r.disp, r.drecv, r.d_ss, r.d_rs)
    moe_compact(a, r)
    moe_gather_start(a, r)
    for i in (1, 2, 3):
        moe_gather_forward(a, r, i)
    moe_gather_finish(a, r)
    moe_experts(a, r)
    moe_pair_start(a, r)
    for i in range(NY):
        moe_pair_sum(a, r, i)
    moe_return_start(a, r)
    moe_combine(a, r)
    moe_finish(a, r, r.out)


def mix_kernel(*refs):
    r = bind((*MIX_IN, "out", *MIX_SCRATCH), refs)
    a = here()
    barrier = pltpu.get_barrier_semaphore()
    for d in (1, 2, 3):
        pl.semaphore_signal(barrier, inc=1, device_id={"x": around(a.x, d, NX)}, device_id_type=MESH_ID)
    for d in (1, -1):
        pl.semaphore_signal(barrier, inc=1, device_id={"z": around(a.z, d, NZ)}, device_id_type=MESH_ID)
    for d in range(1, NY):
        pl.semaphore_signal(barrier, inc=1, device_id={"y": around(a.y, d, NY)}, device_id_type=MESH_ID)
    pl.semaphore_signal(barrier, inc=1, device_id={"c": 1 - a.c}, device_id_type=MESH_ID)
    mix_turn(a, r)
    pl.semaphore_wait(barrier, 13)
    mix_send(a, r)
    for s in range(4):
        mix_step(a, r, s)
        if s == 0:
            for d in (1, 2, 3):
                q_copy(a, r, d).wait_recv()
        if s < 3:
            mix_all_rows(a, r)
    mix_last_rows(a, r)
    mix_combine(a, r)
    mix_project(a, r)
    mix_scatter(a, r)
    mix_sum(a, r)
    mix_finish(a, r, r.out)


def call(kernel, ins, hbm, scratch, out_shape, collective_id, flops):
    n = len(ins) - hbm
    return pl.pallas_call(
        kernel,
        out_shape=out_shape,
        in_specs=[pl.BlockSpec(memory_space=pltpu.VMEM)] * n + [pl.BlockSpec(memory_space=pl.ANY)] * hbm,
        out_specs=pl.BlockSpec(memory_space=pltpu.VMEM),
        scratch_shapes=list(scratch.values()),
        compiler_params=pltpu.CompilerParams(
            collective_id=collective_id, has_side_effects=True, vmem_limit_bytes=60 * 2**20
        ),
        cost_estimate=pl.CostEstimate(flops=flops, bytes_accessed=2**23, transcendentals=0),
    )(*ins)


def turn_tables():
    freq = (THETA ** (-np.arange(0, 64, 2, dtype=np.float32) / np.float32(64))).astype(np.float32)
    row = np.arange(192, dtype=np.float32)[:, None] * freq[None]
    col = np.arange(64, dtype=np.float32)[:, None] * freq[None]
    rowcs = np.zeros((2, 192, 128), np.float32)
    colcs = np.zeros((2, 64, 128), np.float32)
    rowcs[0, :, 0:32] = rowcs[0, :, 32:64] = np.cos(row)
    rowcs[1, :, 0:32], rowcs[1, :, 32:64] = -np.sin(row), np.sin(row)
    colcs[0, :, 64:96] = colcs[0, :, 96:128] = np.cos(col)
    colcs[1, :, 64:96], colcs[1, :, 96:128] = -np.sin(col), np.sin(col)
    return jnp.asarray(rowcs), jnp.asarray(colcs)


def slots_of(ids):
    flat = ids.reshape(-1)
    n = flat.shape[0]
    same = (flat[:, None] == flat[None, :]) & (iota((n, n), 1) < iota((n, n), 0))
    rank = jnp.sum(same.astype(jnp.int32), axis=1)
    return (flat * SLAB + rank).reshape(ids.shape)


def per_device(
    query_rows,
    key_rows,
    value_rows,
    query_gain,
    key_gain,
    w_out,
    mixer_gain,
    expert_input,
    expert_ids,
    expert_weights,
    input_gain,
    w_gate,
    w_up,
    w_down,
    out_gain,
):
    slots = slots_of(expert_ids)
    rowcs, colcs = turn_tables()
    scale = np.float32(np.log2(np.e) * HEAD**-0.5)
    moe_ins = (
        expert_input,
        slots.T,
        slots,
        expert_weights,
        input_gain.reshape(1, D),
        out_gain.reshape(1, 128),
        w_gate[0],
        w_up[0],
        w_down[0],
    )
    moe = call(
        moe_kernel, moe_ins, 3, MOE_SCRATCH, jax.ShapeDtypeStruct((TOKENS2, 128), BF16), 0, 2 * 10**9
    )
    mix_ins = (
        query_rows,
        key_rows,
        value_rows,
        (query_gain * scale).reshape(1, HEAD),
        key_gain.reshape(1, HEAD),
        rowcs,
        colcs,
        mixer_gain.reshape(1, D),
        w_out,
    )
    mix = call(mix_kernel, mix_ins, 1, MIX_SCRATCH, jax.ShapeDtypeStruct((24, D), BF16), 1, 10**10)
    return (mix, moe)


def solution(mesh):
    finer = Mesh(mesh.devices.reshape(NZ, NX, NY, NC), ("z", "x", "y", "c"))
    in_specs = (
        P(EP, TP),
        P(EP, TP),
        P(EP, TP),
        P(),
        P(),
        P(TP, None),
        P(),
        P(EP, None),
        P(EP, None),
        P(EP, None),
        P(),
        P(EP, None, TP),
        P(EP, None, TP),
        P(EP, TP, None),
        P(TP),
    )
    out_specs = (P(EP + TP, None), P(EP, TP))
    return jax.shard_map(
        per_device, mesh=finer, in_specs=in_specs, out_specs=out_specs, check_vma=False
    )
```

time: 288 us -> 172 us (0.60)
  Pallas kernels: 0 us -> 165 us
  waiting for transfers between devices: 78.9 us -> 0 us
  matrix products: 75.5 us -> 0 us
  blocking collectives: 40.6 us -> 0 us
  local copies, waits for them, and re-layouts: 33.1 us -> 5.37 us
  other arithmetic: 23.6 us -> 0.77 us
  starting transfers between devices: 19.5 us -> 0 us
  between operations: 14.2 us -> 0.72 us
    pallas_call x0 -> x2, Pallas kernels: none -> 165 us  [call(): pl.pallas_call(kernel, out_shape=out_shape, in_specs=[pl.BlockSpec(memory...]
    dot_general x51 -> x0, matrix products: 75.5 us -> none  [the longest x24 34.5 us: attend_block(): jnp.einsum('gqn,ngd->gqd', exponent.astype(jnp.bfloat16), value_block, pr...]
    all_to_all x3 -> x0, waiting for transfers between devices: 59.4 us -> none  [the longest x1 49.1 us: sent_to_all(): lax.all_to_all(jnp.broadcast_to(shard[None], (count, *shard.shape)), axis...]
    all_to_all x2 -> x0, blocking collectives: 40.6 us -> none  [the longest x1 24.6 us: expert_half(): lax.all_to_all(outgoing, 'ep', split_axis=0, concat_axis=0, tiled=True)]
    reduce_scatter x2 -> x0, waiting for transfers between devices: 19.5 us -> none  [sum_by_axis(): running = lax.psum_scatter(running, axis, scatter_dimension=0, tiled=True)]
    all_to_all x3 -> x0, starting transfers between devices: 19.3 us -> none  [the longest x1 10.2 us: sent_to_all(): lax.all_to_all(jnp.broadcast_to(shard[None], (count, *shard.shape)), axis...]
    split x3 -> x0, local copies, waits for them, and re-layouts: 15.5 us -> none  [sent_together(): jnp.split(lax.all_gather(both, axis, axis=dim, tiled=True), ends, axis=al...]
    reduce_sum x33 -> x1, other arithmetic: 11.3 us -> 0.24 us  [slots_of(): rank = jnp.sum(same.astype(jnp.int32), axis=1)]
  transfers between devices with their start and end apart: 6 -> 0, of which waited for: 3 -> 0; matrix products, arithmetic and copies ran while one was open for 43% -> 0% of each run, Pallas kernels for 0% -> 0%
where the time goes in v1:
time: 172 us
  Pallas kernels  165 us (96%)
  local copies, waits for them, and re-layouts  5.37 us (3%)
    pallas_call x2, Pallas kernels, call(): pl.pallas_call(kernel, out_shape=out_shape, in_specs=[pl.BlockSpec(memory...  165 us
    unnamed x14, local copies, waits for them, and re-layouts  4.31 us

profile of v1, /device:TPU:1, one launch (start us, length us, event | category | flops | bytes accessed | tf_op | source)
XLA Modules:
  0.0 171.6 jit_solution(8784198732341160890)
XLA Ops:
  0.6 0.8 copy.33
  1.4 0.1 eq.15
  1.6 0.2 convert_reduce_fusion
  1.8 0.0 copy-start.2
  1.8 0.1 reduce_sum.12
  2.0 0.5 copy-done.2
  2.5 0.1 copy.34
  2.7 0.0 copy-start
  2.7 0.0 copy-start.3
  2.7 0.7 copy.35.refs_1_
  3.3 0.0 copy-done.3
  3.4 0.8 copy.36.refs_3_
  4.1 0.0 copy-done
  4.1 0.0 copy-start.4
  4.1 96.5 %shard_map.177 = bf16[192,128]{1,0:T(8,128)(2,1)} custom-call(bf16[192,2048]{1,0:T(8,128)(2,1)} %refs_0_.3, s32[2,192]{1,0:T(2,128)} %copy.35.refs_1_, s32[192,2]{1,0:T(8,128)} %copy-done, f32[192,2]{1,0:T(8,128)} %copy.36.refs_3_, f32[1,2048]{1,0:T(1,128)} %bitcast.14, f32[1,128]{1,0:T(1,128)} %bitcast.16, bf16[2048,256]{1,0:T(8,128)(2,1)} %bitcast.11, ...), custom_call_target="tpu_custom_call" | custom-call | flops 2000000000 | bytes 8388608 | tf_op jit(solution)/shard_map/pallas_call | solution.py:653
  100.6 0.0 copy-done.4
  100.6 0.5 multiply_bitcast_fusion.refs_3_
  101.1 68.3 %shard_map.176 = bf16[24,2048]{1,0:T(8,128)(2,1)} custom-call(bf16[384,256]{1,0:T(8,128)(2,1)} %refs_0_.2, bf16[384,128]{1,0:T(8,128)(2,1)} %refs_1_.1, bf16[384,128]{1,0:T(8,128)(2,1)} %refs_2_.1, f32[1,128]{1,0:T(1,128)} %multiply_bitcast_fusion.refs_3_, f32[1,128]{1,0:T(1,128)} %bitcast.17, f32[2,192,128]{2,1,0:T(8,128)} %constant.10.clone.refs_5_, ...), custom_call_target="tpu_custom_call" | custom-call | flops 10000000000 | bytes 8388608 | tf_op jit(solution)/shard_map/pallas_call | solution.py:653
  169.4 0.0 copy-start.1
  169.4 1.6 copy.39
  171.0 0.0 copy-done.1
  171.0 0.6 copy.40
  (2 shorter events, 0.0 us)
Async XLA Ops:
  1.8 0.7 copy-start.2
  2.7 1.5 copy-start
  2.7 0.7 copy-start.3
  4.1 96.5 %copy-start.4 = (f32[128]{0:T(128)S(1)}, f32[128]{0:T(128)}, u32[]{:S(2)}) copy-start(f32[128]{0:T(128)} %param.20) | copy-start | bytes 1540
  169.4 1.6 copy-start.1

commit v2 on v1

--- a/solution.py
+++ b/solution.py
@@ -24,11 +24,14 @@
 SLOTS = EXPERTS * CAP
 PADDED = EXPERTS * SLAB
 EPS = 1e-06
+SCALE = float(np.log2(np.e) * HEAD**-0.5)
 THETA = 10000.0
 F32 = jnp.float32
 BF16 = jnp.bfloat16
 MESH_ID = pl.DeviceIdType.MESH
-FAR_FIRST = (4, 3, 5, 2, 6, 1, 7, 0)
+PAIR_ORDER = (3, -3, 4, 1, -1, 2, -2, 0)
+ROLE_TO = (1, -1, 0, 1, -1, 2, -2)
+SENT = 24
 X_ORDER = (2, 1, 3, 0)
 
 
@@ -63,9 +66,9 @@
     lax.fori_loop(1, EXPERTS, one, 0)
 
 
-def greet_tp(a, barrier, cores):
+def greet_tp(a, barrier):
     for d in range(NY):
-        for o in range(cores):
+        for o in range(2):
             if d or o:
                 c = a.c if o == 0 else 1 - a.c
                 pl.semaphore_signal(
@@ -93,7 +96,18 @@
     return jnp.sum(jnp.where(eye128(), row, 0.0), axis=1, keepdims=True)
 
 
-MOE_IN = ("xin", "srow", "scol", "wts", "igain", "ogain", "wg_h", "wu_h", "wd_h")
+def tree_copy(a, src, relay, final, ss, rs, role):
+    to = around(a.y, ROLE_TO[role], NY) if role != 2 else lax.rem(a.y + 2 + 4 * a.c, NY)
+    dst = relay.at[role] if role < 3 else final.at[role - 3]
+    return remote(src.at[around(a.y, PAIR_ORDER[role], NY)], dst, ss.at[role], rs.at[role], y=to)
+
+
+def relayed(a, relay, role):
+    share = jnp.where(a.c == 0, 1.0, 0.0) if role == 5 else jnp.where(a.c == 0, 0.0, 1.0)
+    return relay[role - 5].astype(F32) + relay[2].astype(F32) * share
+
+
+MOE_IN = ("xin", "ids", "wts", "igain", "ogain", "wg_h", "wu_h", "wd_h")
 MOE_SCRATCH = dict(
     disp=pltpu.VMEM((EXPERTS, SLAB, 256), BF16),
     drecv=pltpu.VMEM((EXPERTS, SLAB, 256), BF16),
@@ -106,10 +120,12 @@
     pr=pltpu.VMEM((NY, SLOTS, 128), BF16),
     ps=pltpu.VMEM((NY, SLOTS, 128), BF16),
     own=pltpu.VMEM((SLOTS, 128), F32),
-    rs=pltpu.VMEM((NY, SLOTS, 128), BF16),
+    rs=pltpu.VMEM((4, SLOTS, 128), BF16),
+    rl=pltpu.VMEM((3, SLOTS, 128), BF16),
     rsend=pltpu.VMEM((EXPERTS, SLAB, 128), BF16),
     rrecv=pltpu.VMEM((EXPERTS, SLAB, 128), BF16),
     comb=pltpu.VMEM((TOKENS2, 128), F32),
+    scol=pltpu.VMEM((TOKENS2, 2), jnp.int32),
     sqs=pltpu.VMEM((8, 128), F32),
     sqr=pltpu.VMEM((16, 8, 128), F32),
     w_sem=pltpu.SemaphoreType.DMA((3,)),
@@ -140,7 +156,28 @@
         pltpu.make_async_copy(src, dst, r.w_sem.at[i]).wait()
 
 
+def to_cols(row):
+    return jnp.concatenate([to_col(row[:, :128]), to_col(row[:, 64:])[64:]], axis=0)
+
+
+def moe_slots(r):
+    rows = [r.ids[k : k + 1, :].astype(F32) for k in range(2)]
+    cols = [to_cols(v) for v in rows]
+    shape = (TOKENS2, TOKENS2)
+    above, left = iota(shape, 0) < iota(shape, 1), iota(shape, 1) < iota(shape, 0)
+
+    def rank(here, there, mask, dim):
+        hits = [jnp.where((here == v) & mask, 1.0, 0.0) for v in there]
+        return here * SLAB + jnp.sum(hits[0] + hits[1], axis=dim, keepdims=True)
+
+    srow = [rank(v, cols, above, 0).astype(jnp.int32) for v in rows]
+    scol = [rank(v, rows, left, 1).astype(jnp.int32) for v in cols]
+    return srow, scol
+
+
 def moe_dispatch_build(a, r):
+    srow, scol = moe_slots(r)
+    r.scol[...] = jnp.concatenate(scol, axis=1)
     x = r.xin[...].astype(F32)
     inv = lax.rsqrt(jnp.sum(x * x, axis=1, keepdims=True) * (1.0 / D) + EPS)
     g = lax.rem(a.y, 4)
@@ -151,16 +188,20 @@
         halves.append((xs * inv * r.igain[:, pl.ds(off, 128)]).astype(BF16))
     nn = jnp.concatenate(halves, axis=1)
     rows = iota((PADDED, TOKENS2), 0)
-    pick = (rows == r.srow[0:1, :]) | (rows == r.srow[1:2, :])
+    pick = (rows == srow[0]) | (rows == srow[1])
     pick = jnp.where(pick, 1.0, 0.0).astype(BF16)
     out = jnp.dot(pick, nn, preferred_element_type=F32).astype(BF16)
     r.disp[...] = out.reshape(EXPERTS, SLAB, 256)
 
 
+def head(ref, e):
+    return ref.at[e, pl.ds(0, SENT)]
+
+
 def exchange_start(a, src, dst, ss, rs):
     def one(k, carry):
         e, z, x = ep_peer(a, k)
-        remote(src.at[e], dst.at[a.ep], ss, rs, z=z, x=x).start()
+        remote(head(src, e), head(dst, a.ep), ss, rs, z=z, x=x).start()
         return carry
 
     lax.fori_loop(1, EXPERTS, one, 0)
@@ -168,8 +209,8 @@
 
 
 def exchange_wait(src, dst, ss, rs):
-    wait_bytes(dst.at[pl.ds(0, EXPERTS - 1)], rs)
-    wait_bytes(src.at[pl.ds(0, EXPERTS - 1)], ss)
+    wait_bytes(dst.at[pl.ds(0, EXPERTS - 1), pl.ds(0, SENT)], rs)
+    wait_bytes(src.at[pl.ds(0, EXPERTS - 1), pl.ds(0, SENT)], ss)
 
 
 def padded_place(i):
@@ -187,12 +228,10 @@
     r.xg[a.c, g, 1] = out[:, 128:]
 
 
-def moe_gather_copies(a, r):
-    g = lax.rem(a.y, 4)
-    src = r.xg.at[a.c, g]
-    two = around(a.y, 2, NY) + a.c * 4
-    targets = (around(a.y, 1, NY), around(a.y, -1, NY), lax.rem(two, NY))
-    return [remote(src, src, r.ag_ss.at[i], r.ag_rs.at[i], y=t) for i, t in enumerate(targets)]
+def moe_gather_copy(a, r, i):
+    src = r.xg.at[a.c, lax.rem(a.y, 4)]
+    to = around(a.y, (1, -1)[i], NY) if i < 2 else lax.rem(a.y + 2 + 4 * a.c, NY)
+    return remote(src, src, r.ag_ss.at[i], r.ag_rs.at[i], y=to)
 
 
 def moe_group(a, i):
@@ -206,19 +245,19 @@
 
 
 def moe_gather_start(a, r):
-    for cp in moe_gather_copies(a, r):
-        cp.start()
+    for i in range(3):
+        moe_gather_copy(a, r, i).start()
     moe_partner_copy(a, r, 0).start()
 
 
 def moe_gather_forward(a, r, i):
-    moe_gather_copies(a, r)[i - 1].wait_recv()
+    moe_gather_copy(a, r, i - 1).wait_recv()
     moe_partner_copy(a, r, i).start()
 
 
 def moe_gather_finish(a, r):
-    for cp in moe_gather_copies(a, r):
-        cp.wait_send()
+    for i in range(3):
+        moe_gather_copy(a, r, i).wait_send()
     for i in range(4):
         moe_partner_copy(a, r, i).wait()
 
@@ -248,13 +287,12 @@
 
 
 def moe_pair_copy(a, r, i):
-    ys = around(a.y, FAR_FIRST[i], NY)
+    ys = around(a.y, PAIR_ORDER[i], NY)
     return remote(r.part.at[1 - a.c, ys], r.pr.at[ys], r.pp_ss.at[i], r.pp_rs.at[i], c=1 - a.c)
 
 
-def moe_sum_copy(a, r, d):
-    ys = around(a.y, d, NY)
-    return remote(r.ps.at[ys], r.rs.at[d], r.rs_ss.at[d], r.rs_rs.at[d], y=ys)
+def moe_tree_copy(a, r, role):
+    return tree_copy(a, r.ps, r.rl, r.rs, r.rs_ss, r.rs_rs, role)
 
 
 def moe_pair_start(a, r):
@@ -262,23 +300,34 @@
         moe_pair_copy(a, r, i).start()
 
 
-def moe_pair_sum(a, r, i):
-    d = FAR_FIRST[i]
-    ys = around(a.y, d, NY)
+def moe_pair_total(a, r, i):
+    ys = around(a.y, PAIR_ORDER[i], NY)
     moe_pair_copy(a, r, i).wait_recv()
-    total = r.part[a.c, ys].astype(F32) + r.pr[ys].astype(F32)
-    if d:
+    return ys, r.part[a.c, ys].astype(F32) + r.pr[ys].astype(F32)
+
+
+def moe_pair_sums(a, r):
+    for role in range(5):
+        ys, total = moe_pair_total(a, r, role)
         r.ps[ys] = total.astype(BF16)
-        moe_sum_copy(a, r, d).start()
-    else:
-        r.own[...] = total
+        moe_tree_copy(a, r, role).start()
+    r.own[...] = moe_pair_total(a, r, 7)[1]
+
+
+def moe_relay(a, r):
+    moe_tree_copy(a, r, 2).wait_recv()
+    for role in (5, 6):
+        ys, total = moe_pair_total(a, r, role)
+        moe_tree_copy(a, r, role - 5).wait_recv()
+        r.ps[ys] = (total + relayed(a, r.rl, role)).astype(BF16)
+        moe_tree_copy(a, r, role).start()
 
 
 def moe_return_start(a, r):
     total = r.own[...]
-    for d in range(1, NY):
-        moe_sum_copy(a, r, d).wait_recv()
-        total = total + r.rs[d].astype(F32)
+    for role in range(3, 7):
+        moe_tree_copy(a, r, role).wait_recv()
+        total = total + r.rs[role - 3].astype(F32)
     rows = total.astype(BF16)
     place = padded_place(iota((1, SLOTS), 1))
     pick = jnp.where(iota((PADDED, SLOTS), 0) == place, 1.0, 0.0).astype(BF16)
@@ -302,7 +351,7 @@
     total = None
     for k in range(2):
         pick = jnp.where(iota((TOKENS2, PADDED), 1) == r.scol[:, k : k + 1], 1.0, 0.0).astype(BF16)
-        term = jnp.dot(pick, got, preferred_element_type=F32) * r.wts[:, k : k + 1]
+        term = jnp.dot(pick, got, preferred_element_type=F32) * to_cols(r.wts[k : k + 1, :])
         total = term if total is None else total + term
     r.comb[...] = total
     sq = jnp.sum(total * total, axis=1, keepdims=True)
@@ -325,8 +374,8 @@
     lo, hi = to_col(inv[0:1, :]), to_col(inv[1:2, :])
     out[0:128, :] = (r.comb[0:128, :] * lo * r.ogain[...]).astype(BF16)
     out[128:192, :] = (r.comb[128:192, :] * hi[64:] * r.ogain[...]).astype(BF16)
-    for d in range(1, NY):
-        moe_sum_copy(a, r, d).wait_send()
+    for role in range(7):
+        moe_tree_copy(a, r, role).wait_send()
     for i in range(NY):
         moe_pair_copy(a, r, i).wait_send()
 
@@ -349,7 +398,8 @@
     mp=pltpu.VMEM((2, ROWS, 1024), BF16),
     mr=pltpu.VMEM((ROWS, 1024), BF16),
     ms=pltpu.VMEM((NY, 48, 1024), BF16),
-    yr=pltpu.VMEM((NY, 48, 1024), BF16),
+    yr=pltpu.VMEM((4, 48, 1024), BF16),
+    yl=pltpu.VMEM((3, 48, 1024), BF16),
     fs=pltpu.VMEM((48, 1024), F32),
     fr=pltpu.VMEM((24, 1024), F32),
     wo_sem=pltpu.SemaphoreType.DMA,
@@ -393,7 +443,7 @@
     for g in range(ROWS // GRID):
         at = slice(g * GRID, g * GRID + GRID)
         for h in range(2):
-            q = turned(a, r, r.q_in[at, h * 128 : h * 128 + 128], r.qg[...], g)
+            q = turned(a, r, r.q_in[at, h * 128 : h * 128 + 128], r.qg[...] * SCALE, g)
             r.q_all[a.x, h * ROWS + g * GRID : h * ROWS + g * GRID + GRID, :] = q
         keys.append(turned(a, r, r.k_in[at, :], r.kg[...], g))
     key = jnp.concatenate(keys, axis=0)
@@ -482,23 +532,22 @@
     )
 
 
-def mix_last_rows(a, r):
-    for d in X_ORDER:
-        xs = around(a.x, d, NX)
-        dst_o, dst_l = (r.ob, r.lb) if d else (r.orc, r.lrc)
-        for t in range(2 * ROWS // TILE):
-            at = slice(t * TILE, t * TILE + TILE)
-            attend_rows(r, xs, at)
-            acc = r.acc[xs, at, :]
-            total = acc[:, 128:]
-            dst_o[d, at, :] = (acc[:, :128] / total).astype(BF16)
-            lse = r.mx[xs, at, :] + jnp.log2(total)
-            for b in range(TILE // 128):
-                row = t * (TILE // 128) + b
-                dst_l[d, row : row + 1, :] = to_row(lse[b * 128 : b * 128 + 128, :])
-        if d:
-            for cp in part_copies(a, r, d):
-                cp.start()
+def mix_last_rows(a, r, d):
+    xs = around(a.x, d, NX)
+    dst_o, dst_l = (r.ob, r.lb) if d else (r.orc, r.lrc)
+    for t in range(2 * ROWS // TILE):
+        at = slice(t * TILE, t * TILE + TILE)
+        attend_rows(r, xs, at)
+        acc = r.acc[xs, at, :]
+        total = acc[:, 128:]
+        dst_o[d, at, :] = (acc[:, :128] / total).astype(BF16)
+        lse = r.mx[xs, at, :] + jnp.log2(total)
+        for b in range(TILE // 128):
+            row = t * (TILE // 128) + b
+            dst_l[d, row : row + 1, :] = to_row(lse[b * 128 : b * 128 + 128, :])
+    if d:
+        for cp in part_copies(a, r, d):
+            cp.start()
 
 
 def mix_combine(a, r):
@@ -530,9 +579,8 @@
     return remote(r.mp.at[1 - a.c], r.mr, r.m_ss.at[0], r.m_rs.at[0], c=1 - a.c)
 
 
-def mix_sum_copy(a, r, d):
-    y = around(a.y, d, NY)
-    return remote(r.ms.at[y], r.yr.at[d], r.y_ss.at[d], r.y_rs.at[d], y=y)
+def mix_tree_copy(a, r, role):
+    return tree_copy(a, r.ms, r.yl, r.yr, r.y_ss, r.y_rs, role)
 
 
 def mix_project(a, r):
@@ -543,16 +591,27 @@
     mix_pair_copy(a, r).wait_recv()
 
 
+def mix_pair_total(a, r, i):
+    y = around(a.y, PAIR_ORDER[i], NY)
+    at = pl.ds(pl.multiple_of(y * 48, 16), 48)
+    return y, r.mp[a.c, at, :].astype(F32) + r.mr[at, :].astype(F32)
+
+
 def mix_scatter(a, r):
-    for d in FAR_FIRST:
-        y = around(a.y, d, NY)
-        at = pl.ds(pl.multiple_of(y * 48, 16), 48)
-        total = r.mp[a.c, at, :].astype(F32) + r.mr[at, :].astype(F32)
-        if d:
-            r.ms[y] = total.astype(BF16)
-            mix_sum_copy(a, r, d).start()
-        else:
-            r.fs[...] = total
+    for role in range(5):
+        y, total = mix_pair_total(a, r, role)
+        r.ms[y] = total.astype(BF16)
+        mix_tree_copy(a, r, role).start()
+    r.fs[...] = mix_pair_total(a, r, 7)[1]
+
+
+def mix_relay(a, r):
+    mix_tree_copy(a, r, 2).wait_recv()
+    for role in (5, 6):
+        y, total = mix_pair_total(a, r, role)
+        mix_tree_copy(a, r, role - 5).wait_recv()
+        r.ms[y] = (total + relayed(a, r.yl, role)).astype(BF16)
+        mix_tree_copy(a, r, role).start()
 
 
 def mix_final_copy(a, r):
@@ -562,9 +621,9 @@
 
 def mix_sum(a, r):
     total = r.fs[...]
-    for d in range(1, NY):
-        mix_sum_copy(a, r, d).wait_recv()
-        total = total + r.yr[d].astype(F32)
+    for role in range(3, 7):
+        mix_tree_copy(a, r, role).wait_recv()
+        total = total + r.yr[role - 3].astype(F32)
     r.fs[...] = total
     mix_final_copy(a, r).start()
 
@@ -586,80 +645,78 @@
         for cp in kv_copies(a, r, slot):
             cp.wait_send()
     mix_pair_copy(a, r).wait_send()
-    for d in range(1, NY):
-        mix_sum_copy(a, r, d).wait_send()
+    for role in range(7):
+        mix_tree_copy(a, r, role).wait_send()
 
 
 def bind(names, refs):
     return SimpleNamespace(**dict(zip(names, refs, strict=True)))
 
 
-def moe_kernel(*refs):
-    r = bind((*MOE_IN, "out", *MOE_SCRATCH), refs)
+def kernel(*refs):
+    r = bind((*MOE_IN[:-3], *MIX_IN[:-1], *MOE_IN[-3:], MIX_IN[-1], "moe_out", "mix_out", *SCRATCH), refs)
     a = here()
+    r.drecv[...] = jnp.zeros(r.drecv.shape, BF16)
+    r.rrecv[...] = jnp.zeros(r.rrecv.shape, BF16)
     barrier = pltpu.get_barrier_semaphore()
     greet_ep(a, barrier)
-    greet_tp(a, barrier, 2)
+    greet_tp(a, barrier)
     moe_weights(r)
     moe_dispatch_build(a, r)
     pl.semaphore_wait(barrier, 46)
     exchange_start(a, r.disp, r.drecv, r.d_ss, r.d_rs)
+    mix_turn(a, r)
+    mix_send(a, r)
     exchange_wait(r.disp, r.drecv, r.d_ss, r.d_rs)
     moe_compact(a, r)
     moe_gather_start(a, r)
-    for i in (1, 2, 3):
-        moe_gather_forward(a, r, i)
+    mix_step(a, r, 0)
+    for d in (1, 2, 3):
+        q_copy(a, r, d).wait_recv()
+    mix_all_rows(a, r)
+    mix_step(a, r, 1)
+    mix_all_rows(a, r)
+    moe_gather_forward(a, r, 1)
+    moe_gather_forward(a, r, 2)
+    moe_gather_forward(a, r, 3)
+    mix_step(a, r, 2)
     moe_gather_finish(a, r)
     moe_experts(a, r)
     moe_pair_start(a, r)
-    for i in range(NY):
-        moe_pair_sum(a, r, i)
-    moe_return_start(a, r)
-    moe_combine(a, r)
-    moe_finish(a, r, r.out)
-
-
-def mix_kernel(*refs):
-    r = bind((*MIX_IN, "out", *MIX_SCRATCH), refs)
-    a = here()
-    barrier = pltpu.get_barrier_semaphore()
-    for d in (1, 2, 3):
-        pl.semaphore_signal(barrier, inc=1, device_id={"x": around(a.x, d, NX)}, device_id_type=MESH_ID)
-    for d in (1, -1):
-        pl.semaphore_signal(barrier, inc=1, device_id={"z": around(a.z, d, NZ)}, device_id_type=MESH_ID)
-    for d in range(1, NY):
-        pl.semaphore_signal(barrier, inc=1, device_id={"y": around(a.y, d, NY)}, device_id_type=MESH_ID)
-    pl.semaphore_signal(barrier, inc=1, device_id={"c": 1 - a.c}, device_id_type=MESH_ID)
-    mix_turn(a, r)
-    pl.semaphore_wait(barrier, 13)
-    mix_send(a, r)
-    for s in range(4):
-        mix_step(a, r, s)
-        if s == 0:
-            for d in (1, 2, 3):
-                q_copy(a, r, d).wait_recv()
-        if s < 3:
-            mix_all_rows(a, r)
-    mix_last_rows(a, r)
+    mix_all_rows(a, r)
+    moe_pair_sums(a, r)
+    mix_step(a, r, 3)
+    mix_last_rows(a, r, 2)
+    mix_last_rows(a, r, 1)
+    moe_relay(a, r)
+    mix_last_rows(a, r, 3)
+    mix_last_rows(a, r, 0)
     mix_combine(a, r)
     mix_project(a, r)
     mix_scatter(a, r)
+    moe_return_start(a, r)
+    mix_relay(a, r)
+    moe_combine(a, r)
     mix_sum(a, r)
-    mix_finish(a, r, r.out)
-
-
-def call(kernel, ins, hbm, scratch, out_shape, collective_id, flops):
+    moe_finish(a, r, r.moe_out)
+    mix_finish(a, r, r.mix_out)
+
+
+SCRATCH = MOE_SCRATCH | MIX_SCRATCH
+
+
+def call(ins, hbm):
     n = len(ins) - hbm
     return pl.pallas_call(
         kernel,
-        out_shape=out_shape,
+        out_shape=(jax.ShapeDtypeStruct((TOKENS2, 128), BF16), jax.ShapeDtypeStruct((24, D), BF16)),
         in_specs=[pl.BlockSpec(memory_space=pltpu.VMEM)] * n + [pl.BlockSpec(memory_space=pl.ANY)] * hbm,
-        out_specs=pl.BlockSpec(memory_space=pltpu.VMEM),
-        scratch_shapes=list(scratch.values()),
+        out_specs=(pl.BlockSpec(memory_space=pltpu.VMEM),) * 2,
+        scratch_shapes=list(SCRATCH.values()),
         compiler_params=pltpu.CompilerParams(
-            collective_id=collective_id, has_side_effects=True, vmem_limit_bytes=60 * 2**20
+            collective_id=0, has_side_effects=True, vmem_limit_bytes=60 * 2**20
         ),
-        cost_estimate=pl.CostEstimate(flops=flops, bytes_accessed=2**23, transcendentals=0),
+        cost_estimate=pl.CostEstimate(flops=10**10, bytes_accessed=2**23, transcendentals=0),
     )(*ins)
 
 
@@ -674,14 +731,6 @@
     colcs[0, :, 64:96] = colcs[0, :, 96:128] = np.cos(col)
     colcs[1, :, 64:96], colcs[1, :, 96:128] = -np.sin(col), np.sin(col)
     return jnp.asarray(rowcs), jnp.asarray(colcs)
-
-
-def slots_of(ids):
-    flat = ids.reshape(-1)
-    n = flat.shape[0]
-    same = (flat[:, None] == flat[None, :]) & (iota((n, n), 1) < iota((n, n), 0))
-    rank = jnp.sum(same.astype(jnp.int32), axis=1)
-    return (flat * SLAB + rank).reshape(ids.shape)
 
 
 def per_device(
@@ -701,35 +750,29 @@
     w_down,
     out_gain,
 ):
-    slots = slots_of(expert_ids)
     rowcs, colcs = turn_tables()
-    scale = np.float32(np.log2(np.e) * HEAD**-0.5)
-    moe_ins = (
-        expert_input,
-        slots.T,
-        slots,
-        expert_weights,
-        input_gain.reshape(1, D),
-        out_gain.reshape(1, 128),
-        w_gate[0],
-        w_up[0],
-        w_down[0],
+    moe, mix = call(
+        (
+            expert_input,
+            expert_ids.T,
+            expert_weights.T,
+            input_gain.reshape(1, D),
+            out_gain.reshape(1, 128),
+            query_rows,
+            key_rows,
+            value_rows,
+            query_gain.reshape(1, HEAD),
+            key_gain.reshape(1, HEAD),
+            rowcs,
+            colcs,
+            mixer_gain.reshape(1, D),
+            w_gate[0],
+            w_up[0],
+            w_down[0],
+            w_out,
+        ),
+        4,
     )
-    moe = call(
-        moe_kernel, moe_ins, 3, MOE_SCRATCH, jax.ShapeDtypeStruct((TOKENS2, 128), BF16), 0, 2 * 10**9
-    )
-    mix_ins = (
-        query_rows,
-        key_rows,
-        value_rows,
-        (query_gain * scale).reshape(1, HEAD),
-        key_gain.reshape(1, HEAD),
-        rowcs,
-        colcs,
-        mixer_gain.reshape(1, D),
-        w_out,
-    )
-    mix = call(mix_kernel, mix_ins, 1, MIX_SCRATCH, jax.ShapeDtypeStruct((24, D), BF16), 1, 10**10)
     return (mix, moe)
 
 

time: 172 us -> 97.5 us (0.57)
  Pallas kernels: 165 us -> 94.5 us
  local copies, waits for them, and re-layouts: 5.37 us -> 2.18 us
    pallas_call x2 -> x1, Pallas kernels: 165 us -> 94.5 us  [call(): pl.pallas_call(kernel, out_shape=(jax.ShapeDtypeStruct((TOKENS2, 128), BF...]
    unnamed x14 -> x4, local copies, waits for them, and re-layouts: 4.31 us -> 2.18 us
where the time goes in v2:
time: 97.5 us; the launch traced here: 97.3 us
  Pallas kernels  94.5 us (97%)
  local copies, waits for them, and re-layouts  2.18 us (2%)
    pallas_call x1, Pallas kernels, call(): pl.pallas_call(kernel, out_shape=(jax.ShapeDtypeStruct((TOKENS2, 128), BF...  94.5 us
    unnamed x4, local copies, waits for them, and re-layouts  2.18 us

profile of v2, /device:TPU:1, one launch (start us, length us, event | category | flops | bytes accessed | tf_op | source)
XLA Modules:
  0.0 97.3 jit_solution(5477341859559828362)
XLA Ops:
  0.6 94.5 %shard_map.176 = (bf16[192,128]{1,0:T(8,128)(2,1)}, bf16[24,2048]{1,0:T(8,128)(2,1)}) custom-call(bf16[192,2048]{1,0:T(8,128)(2,1)} %refs_0_.1, s32[2,192]{1,0:T(2,128)} %bitcast.15, f32[2,192]{1,0:T(2,128)} %bitcast.16, f32[1,2048]{1,0:T(1,128)} %bitcast.13, f32[1,128]{1,0:T(1,128)} %bitcast.17, bf16[384,256]{1,0:T(8,128)(2,1)} %refs_5_.1, ...), custom_call_target="tpu_custom_call" | custom-call | flops 10000000000 | bytes 8388608 | tf_op jit(solution)/shard_map/pallas_call | solution.py:710
  95.1 0.0 copy-start
  95.2 1.6 %copy.21 = bf16[24,2048]{1,0:T(8,128)(2,1)} copy(bf16[24,2048]{1,0:T(8,128)(2,1)} %get-tuple-element.8) | data formatting | bytes 196608
  96.7 0.0 copy-done
  96.7 0.6 copy.22
Async XLA Ops:
  95.1 1.6 %copy-start = (bf16[192,128]{1,0:T(8,128)(2,1)S(1)}, bf16[192,128]{1,0:T(8,128)(2,1)}, u32[]{:S(2)}) copy-start(bf16[192,128]{1,0:T(8,128)(2,1)} %get-tuple-element.9) | copy-start | bytes 147460

commit v3 on v2

--- a/solution.py
+++ b/solution.py
@@ -32,6 +32,8 @@
 PAIR_ORDER = (3, -3, 4, 1, -1, 2, -2, 0)
 ROLE_TO = (1, -1, 0, 1, -1, 2, -2)
 SENT = 24
+BLOCKS = 3
+BLOCK = 192
 X_ORDER = (2, 1, 3, 0)
 
 
@@ -96,32 +98,33 @@
     return jnp.sum(jnp.where(eye128(), row, 0.0), axis=1, keepdims=True)
 
 
-def tree_copy(a, src, relay, final, ss, rs, role):
+def tree_copy(a, src, relay, final, ss, rs, role, at=()):
     to = around(a.y, ROLE_TO[role], NY) if role != 2 else lax.rem(a.y + 2 + 4 * a.c, NY)
-    dst = relay.at[role] if role < 3 else final.at[role - 3]
-    return remote(src.at[around(a.y, PAIR_ORDER[role], NY)], dst, ss.at[role], rs.at[role], y=to)
-
-
-def relayed(a, relay, role):
+    dst = relay.at[(role, *at)] if role < 3 else final.at[(role - 3, *at)]
+    mine = src.at[(around(a.y, PAIR_ORDER[role], NY), *at)]
+    return remote(mine, dst, ss.at[(*at, role)], rs.at[(*at, role)], y=to)
+
+
+def relayed(a, relay, role, at=()):
     share = jnp.where(a.c == 0, 1.0, 0.0) if role == 5 else jnp.where(a.c == 0, 0.0, 1.0)
-    return relay[role - 5].astype(F32) + relay[2].astype(F32) * share
+    return relay[(role - 5, *at)].astype(F32) + relay[(2, *at)].astype(F32) * share
 
 
 MOE_IN = ("xin", "ids", "wts", "igain", "ogain", "wg_h", "wu_h", "wd_h")
 MOE_SCRATCH = dict(
     disp=pltpu.VMEM((EXPERTS, SLAB, 256), BF16),
     drecv=pltpu.VMEM((EXPERTS, SLAB, 256), BF16),
-    xg=pltpu.VMEM((2, 4, 2, SLOTS, 128), BF16),
-    xcat=pltpu.VMEM((SLOTS, D), BF16),
+    xg=pltpu.VMEM((2, 4, BLOCKS, 2, BLOCK, 128), BF16),
+    xcat=pltpu.VMEM((BLOCK, D), BF16),
     wg=pltpu.VMEM((D, 256), BF16),
     wu=pltpu.VMEM((D, 256), BF16),
     wd=pltpu.VMEM((256, D), BF16),
-    part=pltpu.VMEM((2, NY, SLOTS, 128), BF16),
-    pr=pltpu.VMEM((NY, SLOTS, 128), BF16),
-    ps=pltpu.VMEM((NY, SLOTS, 128), BF16),
-    own=pltpu.VMEM((SLOTS, 128), F32),
-    rs=pltpu.VMEM((4, SLOTS, 128), BF16),
-    rl=pltpu.VMEM((3, SLOTS, 128), BF16),
+    part=pltpu.VMEM((2, NY, BLOCKS, BLOCK, 128), BF16),
+    pr=pltpu.VMEM((NY, BLOCKS, BLOCK, 128), BF16),
+    ps=pltpu.VMEM((NY, BLOCKS, BLOCK, 128), BF16),
+    own=pltpu.VMEM((BLOCKS, BLOCK, 128), F32),
+    rs=pltpu.VMEM((4, BLOCKS, BLOCK, 128), BF16),
+    rl=pltpu.VMEM((3, BLOCKS, BLOCK, 128), BF16),
     rsend=pltpu.VMEM((EXPERTS, SLAB, 128), BF16),
     rrecv=pltpu.VMEM((EXPERTS, SLAB, 128), BF16),
     comb=pltpu.VMEM((TOKENS2, 128), F32),
@@ -131,14 +134,14 @@
     w_sem=pltpu.SemaphoreType.DMA((3,)),
     d_ss=pltpu.SemaphoreType.DMA,
     d_rs=pltpu.SemaphoreType.DMA,
-    ag_ss=pltpu.SemaphoreType.DMA((3,)),
-    ag_rs=pltpu.SemaphoreType.DMA((3,)),
-    pf_ss=pltpu.SemaphoreType.DMA((4,)),
-    pf_rs=pltpu.SemaphoreType.DMA((4,)),
-    pp_ss=pltpu.SemaphoreType.DMA((8,)),
-    pp_rs=pltpu.SemaphoreType.DMA((8,)),
-    rs_ss=pltpu.SemaphoreType.DMA((8,)),
-    rs_rs=pltpu.SemaphoreType.DMA((8,)),
+    ag_ss=pltpu.SemaphoreType.DMA((BLOCKS, 3)),
+    ag_rs=pltpu.SemaphoreType.DMA((BLOCKS, 3)),
+    pf_ss=pltpu.SemaphoreType.DMA((BLOCKS, 4)),
+    pf_rs=pltpu.SemaphoreType.DMA((BLOCKS, 4)),
+    pp_ss=pltpu.SemaphoreType.DMA((BLOCKS, 8)),
+    pp_rs=pltpu.SemaphoreType.DMA((BLOCKS, 8)),
+    rs_ss=pltpu.SemaphoreType.DMA((BLOCKS, 8)),
+    rs_rs=pltpu.SemaphoreType.DMA((BLOCKS, 8)),
     t_ss=pltpu.SemaphoreType.DMA,
     t_rs=pltpu.SemaphoreType.DMA,
     q_ss=pltpu.SemaphoreType.DMA,
@@ -224,111 +227,104 @@
     pick = jnp.where(iota((SLOTS, PADDED), 1) == place, 1.0, 0.0).astype(BF16)
     got = r.drecv[...].reshape(PADDED, 256)
     out = jnp.dot(pick, got, preferred_element_type=F32).astype(BF16)
-    r.xg[a.c, g, 0] = out[:, :128]
-    r.xg[a.c, g, 1] = out[:, 128:]
-
-
-def moe_gather_copy(a, r, i):
-    src = r.xg.at[a.c, lax.rem(a.y, 4)]
+    for b in range(BLOCKS):
+        for h in range(2):
+            r.xg[a.c, g, b, h] = out[b * BLOCK : b * BLOCK + BLOCK, h * 128 : h * 128 + 128]
+
+
+def moe_gather_copy(a, r, b, i):
+    src = r.xg.at[a.c, lax.rem(a.y, 4), b]
     to = around(a.y, (1, -1)[i], NY) if i < 2 else lax.rem(a.y + 2 + 4 * a.c, NY)
-    return remote(src, src, r.ag_ss.at[i], r.ag_rs.at[i], y=to)
+    return remote(src, src, r.ag_ss.at[b, i], r.ag_rs.at[b, i], y=to)
 
 
 def moe_group(a, i):
-    g = lax.rem(a.y, 4)
-    return g if i == 0 else around(g, (3, 1, 2)[i - 1], 4)
-
-
-def moe_partner_copy(a, r, i):
-    src = r.xg.at[a.c, moe_group(a, i)]
-    return remote(src, src, r.pf_ss.at[i], r.pf_rs.at[i], c=1 - a.c)
+    return around(lax.rem(a.y, 4), (0, 3, 1, 2)[i], 4)
+
+
+def moe_partner_copy(a, r, b, i):
+    src = r.xg.at[a.c, moe_group(a, i), b]
+    return remote(src, src, r.pf_ss.at[b, i], r.pf_rs.at[b, i], c=1 - a.c)
 
 
 def moe_gather_start(a, r):
+    for b in range(BLOCKS):
+        for i in (2, 0, 1):
+            moe_gather_copy(a, r, b, i).start()
+    for b in range(BLOCKS):
+        moe_partner_copy(a, r, b, 0).start()
+
+
+def moe_gather_forward(a, r, b):
     for i in range(3):
-        moe_gather_copy(a, r, i).start()
-    moe_partner_copy(a, r, 0).start()
-
-
-def moe_gather_forward(a, r, i):
-    moe_gather_copy(a, r, i - 1).wait_recv()
-    moe_partner_copy(a, r, i).start()
-
-
-def moe_gather_finish(a, r):
-    for i in range(3):
-        moe_gather_copy(a, r, i).wait_send()
+        moe_gather_copy(a, r, b, i).wait_recv()
+        moe_partner_copy(a, r, b, i + 1).start()
+
+
+def moe_experts(a, r, b):
     for i in range(4):
-        moe_partner_copy(a, r, i).wait()
-
-
-def moe_experts(a, r):
+        moe_partner_copy(a, r, b, i).wait_recv()
     for par in range(2):
         for g in range(4):
             for h in range(2):
                 at = ((g + 4 * h) * 2 + par) * 128
-                r.xcat[:, at : at + 128] = r.xg[par, g, h]
-    moe_weights_wait(r)
-
-    def block(b, carry):
-        at = pl.ds(pl.multiple_of(b * 192, 192), 192)
-        xb = r.xcat[at, :]
-        gate = jnp.dot(xb, r.wg[...], preferred_element_type=F32)
-        up = jnp.dot(xb, r.wu[...], preferred_element_type=F32)
-        hid = (gate / (1.0 + jnp.exp(-gate)) * up).astype(BF16)
-        for ys in range(NY):
-            o = jnp.dot(hid, r.wd[:, ys * 256 : ys * 256 + 256], preferred_element_type=F32)
-            o = o.astype(BF16)
-            r.part[0, ys, at, :] = o[:, :128]
-            r.part[1, ys, at, :] = o[:, 128:]
-        return carry
-
-    lax.fori_loop(0, SLOTS // 192, block, 0)
-
-
-def moe_pair_copy(a, r, i):
+                r.xcat[:, at : at + 128] = r.xg[par, g, b, h]
+    if b == 0:
+        moe_weights_wait(r)
+    xb = r.xcat[...]
+    gate = jnp.dot(xb, r.wg[...], preferred_element_type=F32)
+    up = jnp.dot(xb, r.wu[...], preferred_element_type=F32)
+    hid = (gate / (1.0 + jnp.exp(-gate)) * up).astype(BF16)
+    for ys in range(NY):
+        o = jnp.dot(hid, r.wd[:, ys * 256 : ys * 256 + 256], preferred_element_type=F32)
+        o = o.astype(BF16)
+        r.part[0, ys, b] = o[:, :128]
+        r.part[1, ys, b] = o[:, 128:]
+    for i in range(NY):
+        moe_pair_copy(a, r, b, i).start()
+
+
+def moe_pair_copy(a, r, b, i):
     ys = around(a.y, PAIR_ORDER[i], NY)
-    return remote(r.part.at[1 - a.c, ys], r.pr.at[ys], r.pp_ss.at[i], r.pp_rs.at[i], c=1 - a.c)
-
-
-def moe_tree_copy(a, r, role):
-    return tree_copy(a, r.ps, r.rl, r.rs, r.rs_ss, r.rs_rs, role)
-
-
-def moe_pair_start(a, r):
-    for i in range(NY):
-        moe_pair_copy(a, r, i).start()
-
-
-def moe_pair_total(a, r, i):
+    return remote(r.part.at[1 - a.c, ys, b], r.pr.at[ys, b], r.pp_ss.at[b, i], r.pp_rs.at[b, i], c=1 - a.c)
+
+
+def moe_tree_copy(a, r, b, role):
+    return tree_copy(a, r.ps, r.rl, r.rs, r.rs_ss, r.rs_rs, role, (b,))
+
+
+def moe_pair_total(a, r, b, i):
     ys = around(a.y, PAIR_ORDER[i], NY)
-    moe_pair_copy(a, r, i).wait_recv()
-    return ys, r.part[a.c, ys].astype(F32) + r.pr[ys].astype(F32)
-
-
-def moe_pair_sums(a, r):
+    moe_pair_copy(a, r, b, i).wait_recv()
+    return ys, r.part[a.c, ys, b].astype(F32) + r.pr[ys, b].astype(F32)
+
+
+def moe_pair_sums(a, r, b):
     for role in range(5):
-        ys, total = moe_pair_total(a, r, role)
-        r.ps[ys] = total.astype(BF16)
-        moe_tree_copy(a, r, role).start()
-    r.own[...] = moe_pair_total(a, r, 7)[1]
-
-
-def moe_relay(a, r):
-    moe_tree_copy(a, r, 2).wait_recv()
+        ys, total = moe_pair_total(a, r, b, role)
+        r.ps[ys, b] = total.astype(BF16)
+        moe_tree_copy(a, r, b, role).start()
+    r.own[b] = moe_pair_total(a, r, b, 7)[1]
+
+
+def moe_relay(a, r, b):
+    moe_tree_copy(a, r, b, 2).wait_recv()
     for role in (5, 6):
-        ys, total = moe_pair_total(a, r, role)
-        moe_tree_copy(a, r, role - 5).wait_recv()
-        r.ps[ys] = (total + relayed(a, r.rl, role)).astype(BF16)
-        moe_tree_copy(a, r, role).start()
+        ys, total = moe_pair_total(a, r, b, role)
+        moe_tree_copy(a, r, b, role - 5).wait_recv()
+        r.ps[ys, b] = (total + relayed(a, r.rl, role, (b,))).astype(BF16)
+        moe_tree_copy(a, r, b, role).start()
 
 
 def moe_return_start(a, r):
-    total = r.own[...]
-    for role in range(3, 7):
-        moe_tree_copy(a, r, role).wait_recv()
-        total = total + r.rs[role - 3].astype(F32)
-    rows = total.astype(BF16)
+    rows = []
+    for b in range(BLOCKS):
+        total = r.own[b]
+        for role in range(3, 7):
+            moe_tree_copy(a, r, b, role).wait_recv()
+            total = total + r.rs[role - 3, b].astype(F32)
+        rows.append(total.astype(BF16))
+    rows = jnp.concatenate(rows, axis=0)
     place = padded_place(iota((1, SLOTS), 1))
     pick = jnp.where(iota((PADDED, SLOTS), 0) == place, 1.0, 0.0).astype(BF16)
     out = jnp.dot(pick, rows, preferred_element_type=F32).astype(BF16)
@@ -374,10 +370,15 @@
     lo, hi = to_col(inv[0:1, :]), to_col(inv[1:2, :])
     out[0:128, :] = (r.comb[0:128, :] * lo * r.ogain[...]).astype(BF16)
     out[128:192, :] = (r.comb[128:192, :] * hi[64:] * r.ogain[...]).astype(BF16)
-    for role in range(7):
-        moe_tree_copy(a, r, role).wait_send()
-    for i in range(NY):
-        moe_pair_copy(a, r, i).wait_send()
+    for b in range(BLOCKS):
+        for i in range(3):
+            moe_gather_copy(a, r, b, i).wait_send()
+        for i in range(4):
+            moe_partner_copy(a, r, b, i).wait_send()
+        for role in range(7):
+            moe_tree_copy(a, r, b, role).wait_send()
+        for i in range(NY):
+            moe_pair_copy(a, r, b, i).wait_send()
 
 
 MIX_IN = ("q_in", "k_in", "v_in", "qg", "kg", "rowcs", "colcs", "mgain", "wo_h")
@@ -385,34 +386,35 @@
     q_all=pltpu.VMEM((NX, 2 * ROWS, HEAD), BF16),
     kt=pltpu.VMEM((NZ, HEAD, ROWS), BF16),
     va=pltpu.VMEM((NZ, ROWS, HEAD), BF16),
-    kx=pltpu.VMEM((HEAD, 2 * ROWS), BF16),
-    vx=pltpu.VMEM((2 * ROWS, 256), BF16),
+    kx=pltpu.VMEM((2, HEAD, 2 * ROWS), BF16),
+    vx=pltpu.VMEM((2, 2 * ROWS, 256), BF16),
     mx=pltpu.VMEM((NX, 2 * ROWS, 128), F32),
     acc=pltpu.VMEM((NX, 2 * ROWS, 256), F32),
-    ob=pltpu.VMEM((NX, 2 * ROWS, HEAD), BF16),
-    lb=pltpu.VMEM((NX, 8, 128), F32),
-    orc=pltpu.VMEM((NX, 2 * ROWS, HEAD), BF16),
-    lrc=pltpu.VMEM((NX, 8, 128), F32),
-    att=pltpu.VMEM((ROWS, 256), BF16),
-    wo=pltpu.VMEM((256, D), BF16),
-    mp=pltpu.VMEM((2, ROWS, 1024), BF16),
-    mr=pltpu.VMEM((ROWS, 1024), BF16),
+    ob=pltpu.VMEM((NX, 2, ROWS, HEAD), BF16),
+    lb=pltpu.VMEM((NX, 2, 8, 128), F32),
+    orc=pltpu.VMEM((NX, 2, ROWS, HEAD), BF16),
+    lrc=pltpu.VMEM((NX, 2, 8, 128), F32),
+    att=pltpu.VMEM((2, 2, ROWS, HEAD), BF16),
+    wo=pltpu.VMEM((2, 256, 1024), BF16),
+    mp=pltpu.VMEM((ROWS, 1024), F32),
     ms=pltpu.VMEM((NY, 48, 1024), BF16),
     yr=pltpu.VMEM((4, 48, 1024), BF16),
     yl=pltpu.VMEM((3, 48, 1024), BF16),
     fs=pltpu.VMEM((48, 1024), F32),
     fr=pltpu.VMEM((24, 1024), F32),
     wo_sem=pltpu.SemaphoreType.DMA,
+    we_ss=pltpu.SemaphoreType.DMA,
+    we_rs=pltpu.SemaphoreType.DMA,
     xq_ss=pltpu.SemaphoreType.DMA((4,)),
     xq_rs=pltpu.SemaphoreType.DMA((4,)),
     k_ss=pltpu.SemaphoreType.DMA((8,)),
     k_rs=pltpu.SemaphoreType.DMA((8,)),
     v_ss=pltpu.SemaphoreType.DMA((8,)),
     v_rs=pltpu.SemaphoreType.DMA((8,)),
-    o_ss=pltpu.SemaphoreType.DMA((4,)),
-    o_rs=pltpu.SemaphoreType.DMA((4,)),
-    l_ss=pltpu.SemaphoreType.DMA((4,)),
-    l_rs=pltpu.SemaphoreType.DMA((4,)),
+    o_ss=pltpu.SemaphoreType.DMA((4, 2)),
+    o_rs=pltpu.SemaphoreType.DMA((4, 2)),
+    l_ss=pltpu.SemaphoreType.DMA((4, 2)),
+    l_rs=pltpu.SemaphoreType.DMA((4, 2)),
     m_ss=pltpu.SemaphoreType.DMA((2,)),
     m_rs=pltpu.SemaphoreType.DMA((2,)),
     y_ss=pltpu.SemaphoreType.DMA((8,)),
@@ -437,59 +439,70 @@
     return (v * cos + swap_parts(v) * sin).astype(BF16)
 
 
+def column_half(r, half):
+    return r.wo_h.at[:, pl.ds(pl.multiple_of(half * 1024, 1024), 1024)]
+
+
+def own_columns(a, r):
+    return pltpu.make_async_copy(column_half(r, a.c), r.wo.at[a.c], r.wo_sem)
+
+
+def partner_columns(a, r):
+    return remote(column_half(r, 1 - a.c), r.wo.at[a.c], r.we_ss, r.we_rs, c=1 - a.c)
+
+
 def mix_turn(a, r):
-    pltpu.make_async_copy(r.wo_h, r.wo, r.wo_sem).start()
+    own_columns(a, r).start()
     keys = []
     for g in range(ROWS // GRID):
         at = slice(g * GRID, g * GRID + GRID)
         for h in range(2):
             q = turned(a, r, r.q_in[at, h * 128 : h * 128 + 128], r.qg[...] * SCALE, g)
-            r.q_all[a.x, h * ROWS + g * GRID : h * ROWS + g * GRID + GRID, :] = q
+            r.q_all[0, h * ROWS + g * GRID : h * ROWS + g * GRID + GRID, :] = q
         keys.append(turned(a, r, r.k_in[at, :], r.kg[...], g))
     key = jnp.concatenate(keys, axis=0)
     r.kt[OWN] = key.astype(F32).T.astype(BF16)
     r.va[OWN] = r.v_in[...]
-    r.vx[:, 128:] = jnp.ones((2 * ROWS, 128), BF16)
+    r.vx[:, :, 128:] = jnp.ones((2, 2 * ROWS, 128), BF16)
     r.mx[...] = jnp.full(r.mx.shape, -1e30, F32)
     r.acc[...] = jnp.zeros(r.acc.shape, F32)
 
 
 def q_copy(a, r, d):
-    mine = r.q_all.at[a.x]
-    return remote(mine, mine, r.xq_ss.at[d], r.xq_rs.at[d], x=around(a.x, d, NX))
-
-
-def kv_copies(a, r, slot):
+    return remote(r.q_all.at[0], r.q_all.at[NX - d], r.xq_ss.at[d], r.xq_rs.at[d], x=around(a.x, d, NX))
+
+
+def kv_copy(a, r, slot, part):
     src = OWN if slot < 2 else slot - 2
     z = around(a.z, 1 if slot % 2 == 0 else -1, NZ)
-    return (
-        remote(r.kt.at[src], r.kt.at[slot], r.k_ss.at[slot], r.k_rs.at[slot], z=z),
-        remote(r.va.at[src], r.va.at[slot], r.v_ss.at[slot], r.v_rs.at[slot], z=z),
-    )
-
-
-def kv_start(a, r, slot):
-    for cp in kv_copies(a, r, slot):
-        cp.start()
-
-
-def kv_arrived(a, r, slot):
-    for cp in kv_copies(a, r, slot):
-        cp.wait_recv()
-    if slot + 2 < OWN:
-        kv_start(a, r, slot + 2)
+    buf, ss, rs = ((r.kt, r.k_ss, r.k_rs), (r.va, r.v_ss, r.v_rs))[part]
+    return remote(buf.at[src], buf.at[slot], ss.at[slot], rs.at[slot], z=z)
+
+
+def kv_start(a, r, slot, part):
+    kv_copy(a, r, slot, part).start()
+
+
+def kv_arrived(a, r, slots):
+    for part in range(2):
+        for slot in slots:
+            kv_copy(a, r, slot, part).wait_recv()
+            if slot + 2 < OWN:
+                kv_start(a, r, slot + 2, part)
 
 
 def mix_send(a, r):
-    kv_start(a, r, 0)
-    kv_start(a, r, 1)
+    for part in range(2):
+        kv_start(a, r, 0, part)
+        kv_start(a, r, 1, part)
     for d in (2, 1, 3):
         q_copy(a, r, d).start()
 
 
-def attend_rows(r, xs, at):
+def attend_rows(r, s, xs, at):
     q = r.q_all[xs, at, :]
-    s = jnp.dot(q, r.kx[...], preferred_element_type=F32)
+    even = s % 2
+    s = jnp.dot(q, r.kx[even], preferred_element_type=F32)
     old = r.mx[xs, at, :]
     new = jnp.maximum(old, jnp.max(s, axis=1, keepdims=True))
     r.mx[xs, at, :] = new
@@ -497,104 +510,102 @@
         [jnp.exp2(s[:, j * 128 : j * 128 + 128] - new).astype(BF16) for j in range(6)], axis=1
     )
     keep = jnp.exp2(old - new)
-    pv = jnp.dot(p, r.vx[...], preferred_element_type=F32)
+    pv = jnp.dot(p, r.vx[even], preferred_element_type=F32)
     acc = r.acc[xs, at, :]
     r.acc[xs, at, :] = acc * jnp.concatenate([keep, keep], axis=1) + pv
 
 
-TILE = 256
-
-
-def mix_step(a, r, s):
-    slots = (2 * s, 2 * s + 1)
-    for slot in slots:
-        if slot != OWN:
-            kv_arrived(a, r, slot)
-    for i, slot in enumerate(slots):
-        r.kx[:, i * ROWS : i * ROWS + ROWS] = r.kt[slot]
-        r.vx[i * ROWS : i * ROWS + ROWS, :128] = r.va[slot]
-
-
-def mix_all_rows(a, r):
-    def one(xs, carry):
+TILE = 128
+
+
+def mix_arrived(a, r, s):
+    kv_arrived(a, r, [slot for slot in (2 * s, 2 * s + 1) if slot != OWN])
+
+
+def mix_keys(r, s):
+    for i in range(2):
+        r.kx[s % 2, :, i * ROWS : i * ROWS + ROWS] = r.kt[2 * s + i]
+        r.vx[s % 2, i * ROWS : i * ROWS + ROWS, :128] = r.va[2 * s + i]
+
+
+def mix_rows(r, s, targets):
+    for xs in targets:
         for t in range(2 * ROWS // TILE):
-            attend_rows(r, xs, slice(t * TILE, t * TILE + TILE))
-        return carry
-
-    lax.fori_loop(0, NX, one, 0)
-
-
-def part_copies(a, r, d):
+            attend_rows(r, s, xs, slice(t * TILE, t * TILE + TILE))
+
+
+def part_copies(a, r, d, h):
     x = around(a.x, d, NX)
     return (
-        remote(r.ob.at[d], r.orc.at[d], r.o_ss.at[d], r.o_rs.at[d], x=x),
-        remote(r.lb.at[d], r.lrc.at[d], r.l_ss.at[d], r.l_rs.at[d], x=x),
+        remote(r.ob.at[d, h], r.orc.at[d, h], r.o_ss.at[d, h], r.o_rs.at[d, h], x=x),
+        remote(r.lb.at[d, h], r.lrc.at[d, h], r.l_ss.at[d, h], r.l_rs.at[d, h], x=x),
     )
 
 
 def mix_last_rows(a, r, d):
-    xs = around(a.x, d, NX)
+    xs = d
     dst_o, dst_l = (r.ob, r.lb) if d else (r.orc, r.lrc)
-    for t in range(2 * ROWS // TILE):
-        at = slice(t * TILE, t * TILE + TILE)
-        attend_rows(r, xs, at)
-        acc = r.acc[xs, at, :]
-        total = acc[:, 128:]
-        dst_o[d, at, :] = (acc[:, :128] / total).astype(BF16)
-        lse = r.mx[xs, at, :] + jnp.log2(total)
-        for b in range(TILE // 128):
-            row = t * (TILE // 128) + b
-            dst_l[d, row : row + 1, :] = to_row(lse[b * 128 : b * 128 + 128, :])
-    if d:
-        for cp in part_copies(a, r, d):
-            cp.start()
+    for h in range(2):
+        for t in range(ROWS // TILE):
+            at = slice(h * ROWS + t * TILE, h * ROWS + t * TILE + TILE)
+            attend_rows(r, 3, xs, at)
+            acc = r.acc[xs, at, :]
+            total = acc[:, 128:]
+            dst_o[d, h, t * TILE : t * TILE + TILE, :] = (acc[:, :128] / total).astype(BF16)
+            dst_l[d, h, t : t + 1, :] = to_row(r.mx[xs, at, :] + jnp.log2(total))
+        if d:
+            for cp in part_copies(a, r, d, h):
+                cp.start()
+
+
+def mix_heads_copy(a, r, h):
+    mine = r.att.at[a.c, h]
+    return remote(mine, mine, r.m_ss.at[h], r.m_rs.at[h], c=1 - a.c)
 
 
 def mix_combine(a, r):
-    for d in (1, 2, 3):
-        for cp in part_copies(a, r, d):
-            cp.wait_recv()
-    for b in range(6):
-        lse = [to_col(r.lrc[d, b : b + 1, :]) for d in range(NX)]
-        top = functools.reduce(jnp.maximum, lse)
-        w = [jnp.exp2(v - top) for v in lse]
-        inv = 1.0 / functools.reduce(jnp.add, w)
-        at = slice(b * 128, b * 128 + 128)
-        o = None
-        for d in range(NX):
-            term = r.orc[d, at, :].astype(F32) * (w[d] * inv)
-            o = term if o is None else o + term
-        h, t = b // 3, b % 3
-        r.att[t * 128 : t * 128 + 128, h * 128 : h * 128 + 128] = o.astype(BF16)
-
-
-def project(r, half):
+    for h in range(2):
+        for d in (2, 1, 3):
+            for cp in part_copies(a, r, d, h):
+                cp.wait_recv()
+        for t in range(3):
+            lse = [to_col(r.lrc[d, h, t : t + 1, :]) for d in range(NX)]
+            top = functools.reduce(jnp.maximum, lse)
+            w = [jnp.exp2(v - top) for v in lse]
+            inv = 1.0 / functools.reduce(jnp.add, w)
+            at = slice(t * 128, t * 128 + 128)
+            o = None
+            for d in range(NX):
+                term = r.orc[d, h, at, :].astype(F32) * (w[d] * inv)
+                o = term if o is None else o + term
+            r.att[a.c, h, at, :] = o.astype(BF16)
+        mix_heads_copy(a, r, h).start()
+
+
+def project(r, core, j):
+    rows = jnp.concatenate([r.att[core, 0], r.att[core, 1]], axis=1)
+    return jnp.dot(rows, r.wo[core, :, j * 256 : j * 256 + 256], preferred_element_type=F32)
+
+
+def mix_project(a, r):
+    own_columns(a, r).wait()
     for j in range(4):
-        off = pl.multiple_of(half * 1024 + j * 256, 256)
-        o = jnp.dot(r.att[...], r.wo[:, pl.ds(off, 256)], preferred_element_type=F32)
-        r.mp[half, :, j * 256 : j * 256 + 256] = o.astype(BF16)
-
-
-def mix_pair_copy(a, r):
-    return remote(r.mp.at[1 - a.c], r.mr, r.m_ss.at[0], r.m_rs.at[0], c=1 - a.c)
+        r.mp[:, j * 256 : j * 256 + 256] = project(r, a.c, j)
+    partner_columns(a, r).wait_recv()
+    for h in range(2):
+        mix_heads_copy(a, r, h).wait_recv()
+    for j in range(4):
+        r.mp[:, j * 256 : j * 256 + 256] += project(r, 1 - a.c, j)
 
 
 def mix_tree_copy(a, r, role):
     return tree_copy(a, r.ms, r.yl, r.yr, r.y_ss, r.y_rs, role)
-
-
-def mix_project(a, r):
-    pltpu.make_async_copy(r.wo_h, r.wo, r.wo_sem).wait()
-    project(r, 1 - a.c)
-    mix_pair_copy(a, r).start()
-    project(r, a.c)
-    mix_pair_copy(a, r).wait_recv()
 
 
 def mix_pair_total(a, r, i):
     y = around(a.y, PAIR_ORDER[i], NY)
     at = pl.ds(pl.multiple_of(y * 48, 16), 48)
-    return y, r.mp[a.c, at, :].astype(F32) + r.mr[at, :].astype(F32)
+    return y, r.mp[at, :]
 
 
 def mix_scatter(a, r):
@@ -639,12 +650,15 @@
         out[:, off] = (v * inv * r.mgain[:, off]).astype(BF16)
     for d in (1, 2, 3):
         q_copy(a, r, d).wait_send()
-        for cp in part_copies(a, r, d):
-            cp.wait_send()
+        for h in range(2):
+            for cp in part_copies(a, r, d, h):
+                cp.wait_send()
     for slot in range(OWN):
-        for cp in kv_copies(a, r, slot):
-            cp.wait_send()
-    mix_pair_copy(a, r).wait_send()
+        for part in range(2):
+            kv_copy(a, r, slot, part).wait_send()
+    partner_columns(a, r).wait_send()
+    for h in range(2):
+        mix_heads_copy(a, r, h).wait_send()
     for role in range(7):
         mix_tree_copy(a, r, role).wait_send()
 
@@ -663,42 +677,57 @@
     greet_tp(a, barrier)
     moe_weights(r)
     moe_dispatch_build(a, r)
+    mix_turn(a, r)
     pl.semaphore_wait(barrier, 46)
     exchange_start(a, r.disp, r.drecv, r.d_ss, r.d_rs)
-    mix_turn(a, r)
     mix_send(a, r)
+    partner_columns(a, r).start()
     exchange_wait(r.disp, r.drecv, r.d_ss, r.d_rs)
     moe_compact(a, r)
     moe_gather_start(a, r)
-    mix_step(a, r, 0)
+    mix_arrived(a, r, 0)
+    mix_keys(r, 0)
+    mix_rows(r, 0, (0,))
     for d in (1, 2, 3):
         q_copy(a, r, d).wait_recv()
-    mix_all_rows(a, r)
-    mix_step(a, r, 1)
-    mix_all_rows(a, r)
+    mix_rows(r, 0, (1, 2, 3))
+    moe_gather_forward(a, r, 0)
+    mix_arrived(a, r, 1)
+    mix_keys(r, 1)
+    mix_rows(r, 1, (0,))
+    moe_experts(a, r, 0)
     moe_gather_forward(a, r, 1)
+    mix_rows(r, 1, (1,))
+    moe_pair_sums(a, r, 0)
+    moe_experts(a, r, 1)
+    mix_rows(r, 1, (2,))
+    moe_pair_sums(a, r, 1)
     moe_gather_forward(a, r, 2)
-    moe_gather_forward(a, r, 3)
-    mix_step(a, r, 2)
-    moe_gather_finish(a, r)
-    moe_experts(a, r)
-    moe_pair_start(a, r)
-    mix_all_rows(a, r)
-    moe_pair_sums(a, r)
-    mix_step(a, r, 3)
+    mix_arrived(a, r, 2)
+    mix_rows(r, 1, (3,))
+    moe_experts(a, r, 2)
+    mix_keys(r, 2)
+    mix_rows(r, 2, (2,))
+    moe_pair_sums(a, r, 2)
+    moe_relay(a, r, 0)
+    mix_rows(r, 2, (1, 3))
+    moe_relay(a, r, 1)
+    mix_arrived(a, r, 3)
+    mix_keys(r, 3)
     mix_last_rows(a, r, 2)
     mix_last_rows(a, r, 1)
-    moe_relay(a, r)
+    mix_rows(r, 2, (0,))
+    moe_relay(a, r, 2)
     mix_last_rows(a, r, 3)
     mix_last_rows(a, r, 0)
+    moe_return_start(a, r)
     mix_combine(a, r)
     mix_project(a, r)
+    moe_combine(a, r)
     mix_scatter(a, r)
-    moe_return_start(a, r)
+    moe_finish(a, r, r.moe_out)
     mix_relay(a, r)
-    moe_combine(a, r)
     mix_sum(a, r)
-    moe_finish(a, r, r.moe_out)
     mix_finish(a, r, r.mix_out)
 
 

time: 97.5 us -> 92.5 us (0.949)
  Pallas kernels: 94.5 us -> 89.2 us
    pallas_call x1, Pallas kernels: 94.5 us -> 89.2 us  [call(): pl.pallas_call(kernel, out_shape=(jax.ShapeDtypeStruct((TOKENS2, 128), BF...]
where the time goes in v3:
time: 92.5 us; the launch traced here: 92 us
  Pallas kernels  89.2 us (96%)
  local copies, waits for them, and re-layouts  2.18 us (2%)
    pallas_call x1, Pallas kernels, call(): pl.pallas_call(kernel, out_shape=(jax.ShapeDtypeStruct((TOKENS2, 128), BF...  89.2 us
    unnamed x4, local copies, waits for them, and re-layouts  2.18 us

profile of v3, /device:TPU:1, one launch (start us, length us, event | category | flops | bytes accessed | tf_op | source)
XLA Modules:
  0.0 92.0 jit_solution(10412757522797069898)
XLA Ops:
  0.6 89.2 %shard_map.176 = (bf16[192,128]{1,0:T(8,128)(2,1)}, bf16[24,2048]{1,0:T(8,128)(2,1)}) custom-call(bf16[192,2048]{1,0:T(8,128)(2,1)} %refs_0_.1, s32[2,192]{1,0:T(2,128)} %bitcast.15, f32[2,192]{1,0:T(2,128)} %bitcast.16, f32[1,2048]{1,0:T(1,128)} %bitcast.13, f32[1,128]{1,0:T(1,128)} %bitcast.17, bf16[384,256]{1,0:T(8,128)(2,1)} %refs_5_.1, ...), custom_call_target="tpu_custom_call" | custom-call | flops 10000000000 | bytes 8388608 | tf_op jit(solution)/shard_map/pallas_call | solution.py:739
  89.8 0.0 copy-start
  89.8 1.6 %copy.21 = bf16[24,2048]{1,0:T(8,128)(2,1)} copy(bf16[24,2048]{1,0:T(8,128)(2,1)} %get-tuple-element.8) | data formatting | bytes 196608
  91.4 0.0 copy-done
  91.4 0.6 copy.22
Async XLA Ops:
  89.8 1.6 %copy-start = (bf16[192,128]{1,0:T(8,128)(2,1)S(1)}, bf16[192,128]{1,0:T(8,128)(2,1)}, u32[]{:S(2)}) copy-start(bf16[192,128]{1,0:T(8,128)(2,1)} %get-tuple-element.9) | copy-start | bytes 147460

commit v4 on v2

--- a/solution.py
+++ b/solution.py
@@ -32,6 +32,8 @@
 PAIR_ORDER = (3, -3, 4, 1, -1, 2, -2, 0)
 ROLE_TO = (1, -1, 0, 1, -1, 2, -2)
 SENT = 24
+BLOCKS = 3
+BLOCK = 192
 X_ORDER = (2, 1, 3, 0)
 
 
@@ -96,32 +98,33 @@
     return jnp.sum(jnp.where(eye128(), row, 0.0), axis=1, keepdims=True)
 
 
-def tree_copy(a, src, relay, final, ss, rs, role):
+def tree_copy(a, src, relay, final, ss, rs, role, at=()):
     to = around(a.y, ROLE_TO[role], NY) if role != 2 else lax.rem(a.y + 2 + 4 * a.c, NY)
-    dst = relay.at[role] if role < 3 else final.at[role - 3]
-    return remote(src.at[around(a.y, PAIR_ORDER[role], NY)], dst, ss.at[role], rs.at[role], y=to)
-
-
-def relayed(a, relay, role):
+    dst = relay.at[(role, *at)] if role < 3 else final.at[(role - 3, *at)]
+    mine = src.at[(around(a.y, PAIR_ORDER[role], NY), *at)]
+    return remote(mine, dst, ss.at[(*at, role)], rs.at[(*at, role)], y=to)
+
+
+def relayed(a, relay, role, at=()):
     share = jnp.where(a.c == 0, 1.0, 0.0) if role == 5 else jnp.where(a.c == 0, 0.0, 1.0)
-    return relay[role - 5].astype(F32) + relay[2].astype(F32) * share
+    return relay[(role - 5, *at)].astype(F32) + relay[(2, *at)].astype(F32) * share
 
 
 MOE_IN = ("xin", "ids", "wts", "igain", "ogain", "wg_h", "wu_h", "wd_h")
 MOE_SCRATCH = dict(
     disp=pltpu.VMEM((EXPERTS, SLAB, 256), BF16),
     drecv=pltpu.VMEM((EXPERTS, SLAB, 256), BF16),
-    xg=pltpu.VMEM((2, 4, 2, SLOTS, 128), BF16),
-    xcat=pltpu.VMEM((SLOTS, D), BF16),
+    xg=pltpu.VMEM((2, 4, BLOCKS, 2, BLOCK, 128), BF16),
+    xcat=pltpu.VMEM((BLOCK, D), BF16),
     wg=pltpu.VMEM((D, 256), BF16),
     wu=pltpu.VMEM((D, 256), BF16),
     wd=pltpu.VMEM((256, D), BF16),
-    part=pltpu.VMEM((2, NY, SLOTS, 128), BF16),
-    pr=pltpu.VMEM((NY, SLOTS, 128), BF16),
-    ps=pltpu.VMEM((NY, SLOTS, 128), BF16),
-    own=pltpu.VMEM((SLOTS, 128), F32),
-    rs=pltpu.VMEM((4, SLOTS, 128), BF16),
-    rl=pltpu.VMEM((3, SLOTS, 128), BF16),
+    part=pltpu.VMEM((2, NY, BLOCKS, BLOCK, 128), BF16),
+    pr=pltpu.VMEM((NY, BLOCKS, BLOCK, 128), BF16),
+    ps=pltpu.VMEM((NY, BLOCKS, BLOCK, 128), BF16),
+    own=pltpu.VMEM((BLOCKS, BLOCK, 128), F32),
+    rs=pltpu.VMEM((4, BLOCKS, BLOCK, 128), BF16),
+    rl=pltpu.VMEM((3, BLOCKS, BLOCK, 128), BF16),
     rsend=pltpu.VMEM((EXPERTS, SLAB, 128), BF16),
     rrecv=pltpu.VMEM((EXPERTS, SLAB, 128), BF16),
     comb=pltpu.VMEM((TOKENS2, 128), F32),
@@ -131,14 +134,14 @@
     w_sem=pltpu.SemaphoreType.DMA((3,)),
     d_ss=pltpu.SemaphoreType.DMA,
     d_rs=pltpu.SemaphoreType.DMA,
-    ag_ss=pltpu.SemaphoreType.DMA((3,)),
-    ag_rs=pltpu.SemaphoreType.DMA((3,)),
-    pf_ss=pltpu.SemaphoreType.DMA((4,)),
-    pf_rs=pltpu.SemaphoreType.DMA((4,)),
-    pp_ss=pltpu.SemaphoreType.DMA((8,)),
-    pp_rs=pltpu.SemaphoreType.DMA((8,)),
-    rs_ss=pltpu.SemaphoreType.DMA((8,)),
-    rs_rs=pltpu.SemaphoreType.DMA((8,)),
+    ag_ss=pltpu.SemaphoreType.DMA((BLOCKS, 3)),
+    ag_rs=pltpu.SemaphoreType.DMA((BLOCKS, 3)),
+    pf_ss=pltpu.SemaphoreType.DMA((BLOCKS, 4)),
+    pf_rs=pltpu.SemaphoreType.DMA((BLOCKS, 4)),
+    pp_ss=pltpu.SemaphoreType.DMA((BLOCKS, 8)),
+    pp_rs=pltpu.SemaphoreType.DMA((BLOCKS, 8)),
+    rs_ss=pltpu.SemaphoreType.DMA((BLOCKS, 8)),
+    rs_rs=pltpu.SemaphoreType.DMA((BLOCKS, 8)),
     t_ss=pltpu.SemaphoreType.DMA,
     t_rs=pltpu.SemaphoreType.DMA,
     q_ss=pltpu.SemaphoreType.DMA,
@@ -224,111 +227,104 @@
     pick = jnp.where(iota((SLOTS, PADDED), 1) == place, 1.0, 0.0).astype(BF16)
     got = r.drecv[...].reshape(PADDED, 256)
     out = jnp.dot(pick, got, preferred_element_type=F32).astype(BF16)
-    r.xg[a.c, g, 0] = out[:, :128]
-    r.xg[a.c, g, 1] = out[:, 128:]
-
-
-def moe_gather_copy(a, r, i):
-    src = r.xg.at[a.c, lax.rem(a.y, 4)]
+    for b in range(BLOCKS):
+        for h in range(2):
+            r.xg[a.c, g, b, h] = out[b * BLOCK : b * BLOCK + BLOCK, h * 128 : h * 128 + 128]
+
+
+def moe_gather_copy(a, r, b, i):
+    src = r.xg.at[a.c, lax.rem(a.y, 4), b]
     to = around(a.y, (1, -1)[i], NY) if i < 2 else lax.rem(a.y + 2 + 4 * a.c, NY)
-    return remote(src, src, r.ag_ss.at[i], r.ag_rs.at[i], y=to)
+    return remote(src, src, r.ag_ss.at[b, i], r.ag_rs.at[b, i], y=to)
 
 
 def moe_group(a, i):
-    g = lax.rem(a.y, 4)
-    return g if i == 0 else around(g, (3, 1, 2)[i - 1], 4)
-
-
-def moe_partner_copy(a, r, i):
-    src = r.xg.at[a.c, moe_group(a, i)]
-    return remote(src, src, r.pf_ss.at[i], r.pf_rs.at[i], c=1 - a.c)
+    return around(lax.rem(a.y, 4), (0, 3, 1, 2)[i], 4)
+
+
+def moe_partner_copy(a, r, b, i):
+    src = r.xg.at[a.c, moe_group(a, i), b]
+    return remote(src, src, r.pf_ss.at[b, i], r.pf_rs.at[b, i], c=1 - a.c)
 
 
 def moe_gather_start(a, r):
+    for b in range(BLOCKS):
+        for i in (2, 0, 1):
+            moe_gather_copy(a, r, b, i).start()
+    for b in range(BLOCKS):
+        moe_partner_copy(a, r, b, 0).start()
+
+
+def moe_gather_forward(a, r, b):
     for i in range(3):
-        moe_gather_copy(a, r, i).start()
-    moe_partner_copy(a, r, 0).start()
-
-
-def moe_gather_forward(a, r, i):
-    moe_gather_copy(a, r, i - 1).wait_recv()
-    moe_partner_copy(a, r, i).start()
-
-
-def moe_gather_finish(a, r):
-    for i in range(3):
-        moe_gather_copy(a, r, i).wait_send()
+        moe_gather_copy(a, r, b, i).wait_recv()
+        moe_partner_copy(a, r, b, i + 1).start()
+
+
+def moe_experts(a, r, b):
     for i in range(4):
-        moe_partner_copy(a, r, i).wait()
-
-
-def moe_experts(a, r):
+        moe_partner_copy(a, r, b, i).wait_recv()
     for par in range(2):
         for g in range(4):
             for h in range(2):
                 at = ((g + 4 * h) * 2 + par) * 128
-                r.xcat[:, at : at + 128] = r.xg[par, g, h]
-    moe_weights_wait(r)
-
-    def block(b, carry):
-        at = pl.ds(pl.multiple_of(b * 192, 192), 192)
-        xb = r.xcat[at, :]
-        gate = jnp.dot(xb, r.wg[...], preferred_element_type=F32)
-        up = jnp.dot(xb, r.wu[...], preferred_element_type=F32)
-        hid = (gate / (1.0 + jnp.exp(-gate)) * up).astype(BF16)
-        for ys in range(NY):
-            o = jnp.dot(hid, r.wd[:, ys * 256 : ys * 256 + 256], preferred_element_type=F32)
-            o = o.astype(BF16)
-            r.part[0, ys, at, :] = o[:, :128]
-            r.part[1, ys, at, :] = o[:, 128:]
-        return carry
-
-    lax.fori_loop(0, SLOTS // 192, block, 0)
-
-
-def moe_pair_copy(a, r, i):
+                r.xcat[:, at : at + 128] = r.xg[par, g, b, h]
+    if b == 0:
+        moe_weights_wait(r)
+    xb = r.xcat[...]
+    gate = jnp.dot(xb, r.wg[...], preferred_element_type=F32)
+    up = jnp.dot(xb, r.wu[...], preferred_element_type=F32)
+    hid = (gate / (1.0 + jnp.exp(-gate)) * up).astype(BF16)
+    for ys in range(NY):
+        o = jnp.dot(hid, r.wd[:, ys * 256 : ys * 256 + 256], preferred_element_type=F32)
+        o = o.astype(BF16)
+        r.part[0, ys, b] = o[:, :128]
+        r.part[1, ys, b] = o[:, 128:]
+    for i in range(NY):
+        moe_pair_copy(a, r, b, i).start()
+
+
+def moe_pair_copy(a, r, b, i):
     ys = around(a.y, PAIR_ORDER[i], NY)
-    return remote(r.part.at[1 - a.c, ys], r.pr.at[ys], r.pp_ss.at[i], r.pp_rs.at[i], c=1 - a.c)
-
-
-def moe_tree_copy(a, r, role):
-    return tree_copy(a, r.ps, r.rl, r.rs, r.rs_ss, r.rs_rs, role)
-
-
-def moe_pair_start(a, r):
-    for i in range(NY):
-        moe_pair_copy(a, r, i).start()
-
-
-def moe_pair_total(a, r, i):
+    return remote(r.part.at[1 - a.c, ys, b], r.pr.at[ys, b], r.pp_ss.at[b, i], r.pp_rs.at[b, i], c=1 - a.c)
+
+
+def moe_tree_copy(a, r, b, role):
+    return tree_copy(a, r.ps, r.rl, r.rs, r.rs_ss, r.rs_rs, role, (b,))
+
+
+def moe_pair_total(a, r, b, i):
     ys = around(a.y, PAIR_ORDER[i], NY)
-    moe_pair_copy(a, r, i).wait_recv()
-    return ys, r.part[a.c, ys].astype(F32) + r.pr[ys].astype(F32)
-
-
-def moe_pair_sums(a, r):
+    moe_pair_copy(a, r, b, i).wait_recv()
+    return ys, r.part[a.c, ys, b].astype(F32) + r.pr[ys, b].astype(F32)
+
+
+def moe_pair_sums(a, r, b):
     for role in range(5):
-        ys, total = moe_pair_total(a, r, role)
-        r.ps[ys] = total.astype(BF16)
-        moe_tree_copy(a, r, role).start()
-    r.own[...] = moe_pair_total(a, r, 7)[1]
-
-
-def moe_relay(a, r):
-    moe_tree_copy(a, r, 2).wait_recv()
+        ys, total = moe_pair_total(a, r, b, role)
+        r.ps[ys, b] = total.astype(BF16)
+        moe_tree_copy(a, r, b, role).start()
+    r.own[b] = moe_pair_total(a, r, b, 7)[1]
+
+
+def moe_relay(a, r, b):
+    moe_tree_copy(a, r, b, 2).wait_recv()
     for role in (5, 6):
-        ys, total = moe_pair_total(a, r, role)
-        moe_tree_copy(a, r, role - 5).wait_recv()
-        r.ps[ys] = (total + relayed(a, r.rl, role)).astype(BF16)
-        moe_tree_copy(a, r, role).start()
+        ys, total = moe_pair_total(a, r, b, role)
+        moe_tree_copy(a, r, b, role - 5).wait_recv()
+        r.ps[ys, b] = (total + relayed(a, r.rl, role, (b,))).astype(BF16)
+        moe_tree_copy(a, r, b, role).start()
 
 
 def moe_return_start(a, r):
-    total = r.own[...]
-    for role in range(3, 7):
-        moe_tree_copy(a, r, role).wait_recv()
-        total = total + r.rs[role - 3].astype(F32)
-    rows = total.astype(BF16)
+    rows = []
+    for b in range(BLOCKS):
+        total = r.own[b]
+        for role in range(3, 7):
+            moe_tree_copy(a, r, b, role).wait_recv()
+            total = total + r.rs[role - 3, b].astype(F32)
+        rows.append(total.astype(BF16))
+    rows = jnp.concatenate(rows, axis=0)
     place = padded_place(iota((1, SLOTS), 1))
     pick = jnp.where(iota((PADDED, SLOTS), 0) == place, 1.0, 0.0).astype(BF16)
     out = jnp.dot(pick, rows, preferred_element_type=F32).astype(BF16)
@@ -374,10 +370,15 @@
     lo, hi = to_col(inv[0:1, :]), to_col(inv[1:2, :])
     out[0:128, :] = (r.comb[0:128, :] * lo * r.ogain[...]).astype(BF16)
     out[128:192, :] = (r.comb[128:192, :] * hi[64:] * r.ogain[...]).astype(BF16)
-    for role in range(7):
-        moe_tree_copy(a, r, role).wait_send()
-    for i in range(NY):
-        moe_pair_copy(a, r, i).wait_send()
+    for b in range(BLOCKS):
+        for i in range(3):
+            moe_gather_copy(a, r, b, i).wait_send()
+        for i in range(4):
+            moe_partner_copy(a, r, b, i).wait_send()
+        for role in range(7):
+            moe_tree_copy(a, r, b, role).wait_send()
+        for i in range(NY):
+            moe_pair_copy(a, r, b, i).wait_send()
 
 
 MIX_IN = ("q_in", "k_in", "v_in", "qg", "kg", "rowcs", "colcs", "mgain", "wo_h")
@@ -473,11 +474,12 @@
         cp.start()
 
 
-def kv_arrived(a, r, slot):
-    for cp in kv_copies(a, r, slot):
-        cp.wait_recv()
-    if slot + 2 < OWN:
-        kv_start(a, r, slot + 2)
+def kv_arrived(a, r, slots):
+    for part in range(2):
+        for slot in slots:
+            kv_copies(a, r, slot)[part].wait_recv()
+            if slot + 2 < OWN:
+                kv_copies(a, r, slot + 2)[part].start()
 
 
 def mix_send(a, r):
@@ -507,21 +509,19 @@
 
 def mix_step(a, r, s):
     slots = (2 * s, 2 * s + 1)
-    for slot in slots:
-        if slot != OWN:
-            kv_arrived(a, r, slot)
+    kv_arrived(a, r, [slot for slot in slots if slot != OWN])
     for i, slot in enumerate(slots):
         r.kx[:, i * ROWS : i * ROWS + ROWS] = r.kt[slot]
         r.vx[i * ROWS : i * ROWS + ROWS, :128] = r.va[slot]
 
 
-def mix_all_rows(a, r):
+def mix_rows(r, lo, hi):
     def one(xs, carry):
         for t in range(2 * ROWS // TILE):
             attend_rows(r, xs, slice(t * TILE, t * TILE + TILE))
         return carry
 
-    lax.fori_loop(0, NX, one, 0)
+    lax.fori_loop(lo, hi, one, 0)
 
 
 def part_copies(a, r, d):
@@ -663,9 +663,9 @@
     greet_tp(a, barrier)
     moe_weights(r)
     moe_dispatch_build(a, r)
+    mix_turn(a, r)
     pl.semaphore_wait(barrier, 46)
     exchange_start(a, r.disp, r.drecv, r.d_ss, r.d_rs)
-    mix_turn(a, r)
     mix_send(a, r)
     exchange_wait(r.disp, r.drecv, r.d_ss, r.d_rs)
     moe_compact(a, r)
@@ -673,30 +673,35 @@
     mix_step(a, r, 0)
     for d in (1, 2, 3):
         q_copy(a, r, d).wait_recv()
-    mix_all_rows(a, r)
+    mix_rows(r, 0, 4)
+    moe_gather_forward(a, r, 0)
     mix_step(a, r, 1)
-    mix_all_rows(a, r)
+    mix_rows(r, 0, 2)
+    moe_experts(a, r, 0)
     moe_gather_forward(a, r, 1)
+    mix_rows(r, 2, 4)
+    moe_pair_sums(a, r, 0)
+    mix_step(a, r, 2)
+    moe_experts(a, r, 1)
     moe_gather_forward(a, r, 2)
-    moe_gather_forward(a, r, 3)
-    mix_step(a, r, 2)
-    moe_gather_finish(a, r)
-    moe_experts(a, r)
-    moe_pair_start(a, r)
-    mix_all_rows(a, r)
-    moe_pair_sums(a, r)
+    mix_rows(r, 0, 2)
+    moe_pair_sums(a, r, 1)
+    moe_experts(a, r, 2)
+    moe_relay(a, r, 0)
+    mix_rows(r, 2, 4)
+    moe_pair_sums(a, r, 2)
     mix_step(a, r, 3)
     mix_last_rows(a, r, 2)
-    mix_last_rows(a, r, 1)
-    moe_relay(a, r)
-    mix_last_rows(a, r, 3)
-    mix_last_rows(a, r, 0)
+    moe_relay(a, r, 1)
+    for d in (1, 3, 0):
+        mix_last_rows(a, r, d)
+    moe_relay(a, r, 2)
+    moe_return_start(a, r)
     mix_combine(a, r)
     mix_project(a, r)
     mix_scatter(a, r)
-    moe_return_start(a, r)
+    moe_combine(a, r)
     mix_relay(a, r)
-    moe_combine(a, r)
     mix_sum(a, r)
     moe_finish(a, r, r.moe_out)
     mix_finish(a, r, r.mix_out)

time: 97.5 us -> 91 us (0.933)
  Pallas kernels: 94.5 us -> 88 us
    pallas_call x1, Pallas kernels: 94.5 us -> 88 us  [call(): pl.pallas_call(kernel, out_shape=(jax.ShapeDtypeStruct((TOKENS2, 128), BF...]
where the time goes in v4:
time: 91 us; the launch traced here: 90.8 us
  Pallas kernels  88 us (97%)
  local copies, waits for them, and re-layouts  2.18 us (2%)
    pallas_call x1, Pallas kernels, call(): pl.pallas_call(kernel, out_shape=(jax.ShapeDtypeStruct((TOKENS2, 128), BF...  88 us
    unnamed x4, local copies, waits for them, and re-layouts  2.18 us

profile of v4, /device:TPU:1, one launch (start us, length us, event | category | flops | bytes accessed | tf_op | source)
XLA Modules:
  0.0 90.8 jit_solution(12068291295584413669)
XLA Ops:
  0.6 88.0 %shard_map.176 = (bf16[192,128]{1,0:T(8,128)(2,1)}, bf16[24,2048]{1,0:T(8,128)(2,1)}) custom-call(bf16[192,2048]{1,0:T(8,128)(2,1)} %refs_0_.1, s32[2,192]{1,0:T(2,128)} %bitcast.15, f32[2,192]{1,0:T(2,128)} %bitcast.16, f32[1,2048]{1,0:T(1,128)} %bitcast.13, f32[1,128]{1,0:T(1,128)} %bitcast.17, bf16[384,256]{1,0:T(8,128)(2,1)} %refs_5_.1, ...), custom_call_target="tpu_custom_call" | custom-call | flops 10000000000 | bytes 8388608 | tf_op jit(solution)/shard_map/pallas_call | solution.py:715
  88.6 0.0 copy-start
  88.6 1.6 %copy.21 = bf16[24,2048]{1,0:T(8,128)(2,1)} copy(bf16[24,2048]{1,0:T(8,128)(2,1)} %get-tuple-element.8) | data formatting | bytes 196608
  90.2 0.0 copy-done
  90.2 0.6 copy.22
Async XLA Ops:
  88.6 1.6 %copy-start = (bf16[192,128]{1,0:T(8,128)(2,1)S(1)}, bf16[192,128]{1,0:T(8,128)(2,1)}, u32[]{:S(2)}) copy-start(bf16[192,128]{1,0:T(8,128)(2,1)} %get-tuple-element.9) | copy-start | bytes 147460
